TPU v7x, 32 devices: a whole 2x2x4 slice. The times are simulated.
32 devices in a mesh: sp: 8 (over z, x), tp: 4 (over y, core).
Axes of the slice: x: 2, y: 2, z: 4, core: 2. Of those that a mesh axis runs over, the one named last changes fastest.
Arguments:
- tokens: bfloat16 [4096, 4096], P(('sp', 'tp')), may hold values from -6 to 6
- lock_projector: bfloat16 [4096, 1024], P(None, 'tp'), may hold values from -0.01171875 to 0.01171875
- value_weight: bfloat16 [4096, 2048], P(None, 'tp'), may hold values from -0.0234375 to 0.0234375
- decay_weight: bfloat16 [4096, 1024], P(None, 'tp'), may hold values from -0.09375 to 0.09375
- decay_offset: float32 [1024], P('tp'), may hold values from -3.5 to 0
- fresh_question: bfloat16 [16, 64], P('tp'), may hold values from -6 to 6
Outputs:
- state_cache: bfloat16 [16, 64, 128], P('tp', 'sp')
- first_read: bfloat16 [16, 128], P('tp')
All inputs are finite; a program needn't handle non-finite values.
Results may differ from a plain program's by a relative error of at most 0.0034.
Values may be sent and summed in bfloat16 or wider, within the bound.
No kernel may reach another device: no remote copies, remote signals or barrier semaphores. Data moves between devices by JAX's collectives and lax.ppermute only.
A program may use at most 64 MiB of HBM per device.

v0:
```python
import math

import jax
import jax.numpy as jnp
from jax import lax
from jax.sharding import PartitionSpec as P

CUE_WIDTH = 64
DV = 128


decay_tau = 16.0


def carried_in(part, axis, combine, identity):
    count = lax.axis_size(axis)
    place = lax.axis_index(axis)
    ahead = count - 1 - place
    gathered = lax.all_gather(part, axis)
    state = jnp.zeros_like(part) + jnp.asarray(identity, part.dtype)

    def one(hop, state):
        source = count - 1 - hop
        return combine(state, lax.dynamic_index_in_dim(gathered, source, 0, False))

    return lax.fori_loop(0, ahead, one, state)


def add_logs(earlier, later_sum):
    return earlier + later_sum


def per_device(tokens, lock_projector, value_weight, decay_weight, decay_offset, fresh_question):
    key_cols = lock_projector.shape[1]
    value_cols = value_weight.shape[1]
    local_heads = key_cols // CUE_WIDTH
    combined = jnp.concatenate([lock_projector, value_weight, decay_weight], axis=1)
    projected = jnp.dot(
        lax.all_gather(tokens, "tp", axis=0, tiled=True),
        combined,
        preferred_element_type=jnp.float32,
    )
    span_rows = projected.shape[0]
    lock_vectors = projected[:, :key_cols].astype(jnp.bfloat16)
    value_rows = projected[:, key_cols : key_cols + value_cols].astype(jnp.bfloat16)
    decay_pre = projected[:, key_cols + value_cols :]
    length = span_rows * lax.axis_size("sp")
    log_decay = jax.nn.log_sigmoid(decay_pre + decay_offset[None, :] + math.log(length)) / decay_tau
    segment_overall = jnp.sum(log_decay, axis=0)
    later_total = carried_in(segment_overall, "sp", add_logs, jnp.zeros_like(segment_overall))
    after = (segment_overall + later_total)[None, :] - jnp.cumsum(log_decay, axis=0)
    weighted = (lock_vectors.astype(jnp.float32) * jnp.exp(after)).astype(jnp.bfloat16)
    lookup_probes = weighted.reshape(span_rows, local_heads, CUE_WIDTH)
    stored_contents = value_rows.reshape(span_rows, local_heads, DV)
    summands_list = jnp.einsum(
        "nyl,nyp->ylp", lookup_probes, stored_contents, preferred_element_type=jnp.float32
    )
    key_scale = CUE_WIDTH ** (-0.5)
    question_widened = fresh_question.astype(jnp.float32)
    row_span = CUE_WIDTH // lax.axis_size("sp")
    row_start = lax.axis_index("sp") * row_span
    recall_grid = lax.psum(summands_list, "sp")
    segment_lines = lax.dynamic_slice_in_dim(recall_grid, row_start, row_span, 1)
    attended_blend = key_scale * jnp.einsum(
        "qw,qwi->qi", question_widened, recall_grid, precision=lax.Precision.HIGHEST
    )
    state_cache = segment_lines.astype(jnp.bfloat16)
    first_read = attended_blend * lax.rsqrt(
        jnp.mean(attended_blend * attended_blend, axis=-1, keepdims=True) + 1.0
    )
    return (state_cache, first_read.astype(jnp.bfloat16))


def solution(mesh):
    in_specs = (
        P(("sp", "tp"), None),
        P(None, "tp"),
        P(None, "tp"),
        P(None, "tp"),
        P("tp"),
        P("tp", None),
    )
    out_specs = (P("tp", "sp", None), P("tp", None))
    return jax.shard_map(
        per_device, mesh=mesh, in_specs=in_specs, out_specs=out_specs, check_vma=False
    )
```

profile of v0, /device:TPU:0, one launch (start us, length us, event | category | flops | bytes accessed | tf_op | source)
XLA Modules:
  0.0 155.6 jit_solution(18224980167365922461)
XLA Ops:
  7.2 0.0 copy-start
  7.2 0.0 all-gather.4.cloned.1.call-start
  7.2 0.7 all-gather.4.cloned.1.call-update
  7.9 0.0 all-reduce.2.cloned.1.call-start
  8.0 0.0 copy-start.1
  8.0 38.8 %all-gather.4.cloned.1.call-done = bf16[512,4096]{1,0:T(8,128)(2,1)} async-done(((bf16[128,4096]{1,0:T(8,128)(2,1)}), bf16[512,4096]{1,0:T(8,128)(2,1)}) %all-gather.4.cloned.1.call-update) | async-done | bytes 4194320 | tf_op jit(solution)/shard_map/all_gather | solution.py:39
  46.8 8.3 %fusion.22 = (bf16[512,1024]{0,1:T(8,128)(2,1)S(1)}, f32[512,1024]{0,1:T(8,128)S(1)}) fusion(bf16[512,4096]{1,0:T(8,128)(2,1)} %all-gather.4.cloned.1.call-done, bf16[4096,256]{1,0:T(8,128)(2,1)} %param.11, bf16[4096,512]{1,0:T(8,128)(2,1)} %param.10, bf16[4096,256]{1,0:T(8,128)(2,1)} %param.9), kind=kOutput, calls=%fused_computation.31 | convolution fusion | flops 4320657408 | bytes 15728640 | tf_op jit(solution)/shard_map/dot_general | solution.py:38
  55.1 0.0 copy-done.1
  55.1 0.5 fusion.21
  55.6 20.5 %all-gather.1 = f32[8,1,256]{2,1,0:T(1,128)S(1)} all-gather(f32[1,1,256]{2,1,0:T(1,128)S(1)} %bitcast.54), channel_id=2, replica_groups=mesh['sp'=8,'tp'=4] {'sp'}, dimensions={0}, use_global_device_ids=true | all-gather | bytes 9216 | tf_op jit(solution)/shard_map/all_gather | solution.py:19
  76.1 0.3 while.12
  76.5 0.2 reshape.30
  76.7 0.2 copy.11
  76.9 0.1 fusion.23
  77.2 0.3 copy.12
  77.5 0.2 fusion.14
  77.6 1.0 fusion.24
  78.6 0.0 all-reduce.2.cloned.1.call-update
  78.6 67.0 %all-reduce.2.cloned.1.call-done = f32[4,64,128]{2,1,0:T(8,128)} async-done(((f32[4,64,128]{2,1,0:T(8,128)}), f32[4,64,128]{2,1,0:T(8,128)}) %all-reduce.2.cloned.1.call-update) | async-done | bytes 131088 | tf_op jit(solution)/shard_map/psum | solution.py:62
  145.6 0.0 copy-done
  145.6 1.1 fusion.17
  146.7 0.1 multiply_reduce_fusion
  146.8 0.6 multiply_convert_fusion
  147.5 1.3 dynamic-slice_convert_fusion
  (24 shorter events, 0.3 us)
Async XLA Ops:
  7.2 138.4 %copy-start = (bf16[4,64]{1,0:T(4,128)(2,1)S(1)}, bf16[4,64]{1,0:T(4,128)(2,1)}, u32[]{:S(2)}) copy-start(bf16[4,64]{1,0:T(4,128)(2,1)} %param.13) | copy-start | bytes 1540
  7.2 39.6 %all-gather.4.cloned.1.call-start = ((), (), s32[]{:S(2)}) async-start(), calls=%async_computation | async-start | bytes 5242880 | tf_op jit(solution)/shard_map/all_gather | solution.py:39
  7.9 137.7 %all-reduce.2.cloned.1.call-start = ((), (), s32[]{:S(2)}) async-start(), calls=%async_computation.1 | async-start | bytes 262144 | tf_op jit(solution)/shard_map/psum | solution.py:62
  8.0 47.1 %copy-start.1 = (f32[256]{0:T(256)S(1)}, f32[256]{0:T(256)}, u32[]{:S(2)}) copy-start(f32[256]{0:T(256)} %param.12) | copy-start | bytes 3076
Sparse Core Ops, SparseCore 0:
  9.5 37.1 all-gather.3
  78.7 66.8 all-reduce.1
where the time goes:
time: 156 us
  waiting for transfers between devices  106 us (68%)
  blocking collectives  20.5 us (13%)
  between operations  14.1 us (9%)
  matrix products  10.3 us (7%)
  local copies, waits for them, and re-layouts  2.13 us (1%)
  other arithmetic  1.74 us (1%)
    psum x1, waiting for transfers between devices, per_device(): recall_grid = lax.psum(summands_list, 'sp')  67 us
    all_gather x1, waiting for transfers between devices, per_device(): lax.all_gather(tokens, 'tp', axis=0, tiled=True)  38.8 us
    all_gather x1, blocking collectives, carried_in(): gathered = lax.all_gather(part, axis)  20.5 us
    dot_general x1, matrix products, per_device(): jnp.dot(lax.all_gather(tokens, 'tp', axis=0, tiled=True), combined, prefe...  8.32 us
  transfers between devices with their start and end apart: 2, of which 2 were waited for; matrix products, arithmetic and copies ran while one was open for 0% of the time, Pallas kernels for 0%

commit v1 on v0

v1 whole, which is shorter than its diff:
```python
import functools
import math

import jax
import jax.numpy as jnp
from jax import lax
from jax.experimental import pallas as pl
from jax.experimental.pallas import tpu as pltpu
from jax.sharding import PartitionSpec as P


CUE_WIDTH = 64
DV = 128
DECAY_TAU = 16.0
LATE_PARTS = 4
VMEM_LIMIT = 24 * 1024 * 1024


F32 = jnp.float32
BF16 = jnp.bfloat16
EXACT = lax.Precision.HIGHEST


def swap(count, bit):
    return [(i, i ^ bit) for i in range(count)]


def project(x, wk, wv, wd, offset, log_length):
    keys = jnp.dot(x, wk[...], preferred_element_type=F32).astype(BF16)
    values = jnp.dot(x, wv[...], preferred_element_type=F32).astype(BF16)
    pre = jnp.dot(x, wd[...], preferred_element_type=F32)
    z = pre + offset + log_length
    log_decay = (jnp.minimum(z, 0.0) - jnp.log1p(jnp.exp(-jnp.abs(z)))) / DECAY_TAU
    return keys, values, log_decay


def later_within(log_decay, blocks):
    rows = log_decay.shape[0]
    size = rows // blocks
    i = lax.broadcasted_iota(jnp.int32, (rows, rows), 0)
    j = lax.broadcasted_iota(jnp.int32, (rows, rows), 1)
    mask = j > i
    for b in range(1, blocks):
        mask = mask & ((i >= b * size) == (j >= b * size))
    return jnp.dot(mask.astype(F32), log_decay, precision=EXACT, preferred_element_type=F32)


def weigh(keys, after):
    exact = keys.astype(F32) * jnp.exp(after)
    high = exact.astype(BF16)
    return high, (exact - high.astype(F32)).astype(BF16)


def outer(values, weighted):
    high, low = weighted
    heads = high.shape[1] // CUE_WIDTH
    group = min(2, heads)
    cols = group * CUE_WIDTH
    parts = []
    for g in range(heads // group):
        w = jnp.concatenate([p[:, g * cols : (g + 1) * cols] for p in (high, low)], axis=1)
        v = values[:, g * group * DV : (g + 1) * group * DV]
        full = lax.dot_general(v, w, (((0,), (0,)), ((), ())), preferred_element_type=F32)
        full = full[:, :cols] + full[:, cols:]
        kept = full[:DV]
        if group == 2:
            lane = lax.broadcasted_iota(jnp.int32, kept.shape, 1)
            kept = jnp.where(lane < CUE_WIDTH, kept, full[DV:])
        parts.append(kept)
    return parts[0] if len(parts) == 1 else jnp.concatenate(parts, axis=1)


def payload_sds(heads):
    pad = -(3 + 3 * heads) % 16
    width = max(heads * CUE_WIDTH, DV)
    return jax.ShapeDtypeStruct((DV + 3 + 3 * heads + pad, width), BF16)


def split(exact):
    parts, rest = [], exact
    for _ in range(3):
        parts.append(rest.astype(BF16).astype(F32))
        rest = rest - parts[-1]
    return parts


def widen(x, width):
    extra = width - x.shape[1]
    return jnp.concatenate([x, jnp.zeros((x.shape[0], extra), x.dtype)], axis=1) if extra else x


def pack(out, state, total, heard=None):
    width = out.shape[1]
    rows = [widen(p, width) for p in split(total)]
    if heard is not None:
        for part in split(heard):
            part = widen(part, width)
            rows += [part[h : h + 1] for h in range(part.shape[0])]
    row = lax.broadcasted_iota(jnp.int32, (out.shape[0] - DV, width), 0)
    tail = jnp.zeros(row.shape, F32)
    for n, value in enumerate(rows):
        tail = jnp.where(row == n, value, tail)
    out[:DV, :] = widen(state.astype(BF16), width)
    out[DV:, :] = tail.astype(BF16)


def unpack(ref, key_cols):
    tail = ref[DV:, :].astype(F32)
    total = tail[0:1] + tail[1:2] + tail[2:3]
    return ref[:DV, :key_cols].astype(F32), total[:, :key_cols], tail


def heard_of(tail, heads):
    parts = [tail[3 + n * heads : 3 + (n + 1) * heads, :DV] for n in range(3)]
    return parts[0] + parts[1] + parts[2]


def asking(question, rows):
    row = lax.broadcasted_iota(jnp.int32, (rows, question.shape[1]), 0)
    lane = lax.broadcasted_iota(jnp.int32, (rows, question.shape[1]), 1)
    asked = question[...].astype(F32) * CUE_WIDTH ** (-0.5)
    return jnp.where(lax.div(lane, CUE_WIDTH) == row, asked, 0.0)


def against(left, state):
    return lax.dot_general(
        left, state, (((1,), (1,)), ((), ())), precision=EXACT, preferred_element_type=F32
    )


def near_kernel(x0, x1, wk, wv, wd, off, s_out, l_out, *, log_length):
    core = lax.rem(lax.axis_index("tp"), 2)
    rows = x0.shape[0]
    x = jnp.concatenate([x0[...], x1[...]], axis=0)
    keys, values, log_decay = project(x, wk, wv, wd, off[...], log_length)
    after = later_within(log_decay, 2)
    own = after[0:1] + log_decay[0:1]
    sib = after[rows : rows + 1] + log_decay[rows : rows + 1]
    own_tail = jnp.where(core == 0, sib, 0.0)
    sib_tail = jnp.where(core == 0, 0.0, own)
    row = lax.broadcasted_iota(jnp.int32, after.shape, 0)
    after = after + jnp.where(row < rows, own_tail, sib_tail)
    s_out[...] = outer(values, weigh(keys, after))
    l_out[...] = own + sib


def early_kernel(xa, xb, wk, wv, wd, off, s_a, s_b, l_a, l_b, *, log_length):
    rows = xa.shape[0]
    x = jnp.concatenate([xa[...], xb[...]], axis=0)
    keys, values, log_decay = project(x, wk, wv, wd, off[...], log_length)
    after = later_within(log_decay, 2)
    weighted = weigh(keys, after)
    s_a[...] = outer(values[:rows], [w[:rows] for w in weighted])
    s_b[...] = outer(values[rows:], [w[rows:] for w in weighted])
    l_a[...] = after[0:1] + log_decay[0:1]
    l_b[...] = after[rows : rows + 1] + log_decay[rows : rows + 1]


def late_kernel(xa, xb, wk, wv, wd, off, *refs, log_length, blocks, here, parts):
    states = refs[: len(blocks)]
    totals = refs[len(blocks) : 2 * len(blocks)]
    out = refs[2 * len(blocks)]
    place = lax.axis_index("tp")
    core = lax.rem(place, 2)
    chip = lax.div(place, 2)
    rows = xa.shape[0]

    def position(block):
        if block is None:
            return chip * (2 * parts)
        bit, part, same = block
        parity = core if same else 1 - core
        return lax.bitwise_xor(chip, bit) * (2 * parts) + parity * parts + part

    x = jnp.concatenate([xa[...], xb[...]], axis=0)
    keys, values, log_decay = project(x, wk, wv, wd, off[...], log_length)
    after = later_within(log_decay, 2)
    own = [
        after[0:1] + log_decay[0:1],
        after[rows : rows + 1] + log_decay[rows : rows + 1],
    ]
    every = [(position(b), totals[n][...]) for n, b in enumerate(blocks)]
    mine = [position(here + (True,)), position(here + (False,))]
    every += list(zip(mine, own))

    def later_of(pos):
        acc = jnp.zeros_like(own[0])
        for p, t in every:
            acc = acc + jnp.where(p > pos, t, 0.0)
        return acc

    row = lax.broadcasted_iota(jnp.int32, after.shape, 0)
    after = after + jnp.where(row < rows, later_of(mine[0]), later_of(mine[1]))
    state = outer(values, weigh(keys, after))
    total = own[0] + own[1]
    for n in range(len(blocks)):
        pos, t = every[n]
        state = state + states[n][...] * jnp.exp(later_of(pos))
        total = total + t
    pack(out, state, total)


def merge_kernel(question, *refs, bits):
    count = 2 ** len(bits)
    out, exact = refs[count:]
    key_cols = question.shape[1]
    parts = [unpack(ref, key_cols)[:2] for ref in refs[:count]]
    for n, bit in enumerate(bits):
        turned = lax.bitwise_and(lax.axis_index("sp"), bit) != 0
        parts = [
            tuple(jnp.where(turned, x, y) for x, y in zip(parts[k ^ (1 << n)], parts[k]))
            for k in range(count)
        ]
    state, total = parts[0]
    for s, t in parts[1:]:
        state = state * jnp.exp(t) + s
        total = total + t
    exact[...] = state
    heads = key_cols // CUE_WIDTH
    pack(out, state, total, against(asking(question, 8), state)[:heads])


def final_kernel(question, mine, other, exact, cache, read, *, bit):
    heads, kept, _ = cache.shape
    key_cols = question.shape[1]
    earlier = lax.bitwise_and(lax.axis_index("sp"), bit) == 0
    s_m, l_m, tail_m = unpack(mine, key_cols)
    s_o, l_o, tail_o = unpack(other, key_cols)
    fading = jnp.exp(jnp.where(earlier, l_o, l_m))
    first = jnp.where(earlier, s_m, s_o) * fading
    state = jnp.where(earlier, exact[...] * fading + s_o, first + exact[...])
    rows = heads * kept
    rows += -rows % 8
    row = lax.broadcasted_iota(jnp.int32, (rows, key_cols), 0)
    lane = lax.broadcasted_iota(jnp.int32, (rows, key_cols), 1)
    start = lax.axis_index("sp") * kept
    column = lax.div(row, kept) * CUE_WIDTH + start + lax.rem(row, kept)
    chosen = ((row < heads * kept) & (lane == column)).astype(F32)
    result = against(chosen, state)
    for h in range(heads):
        cache[h] = result[h * kept : (h + 1) * kept].astype(BF16)
    heard = against(asking(question, 8), first)[:heads]
    heard = heard + heard_of(jnp.where(earlier, tail_o, tail_m), heads)
    mean = jnp.mean(heard * heard, axis=-1, keepdims=True)
    read[...] = (heard * lax.rsqrt(mean + 1.0)).astype(BF16)


VM = pl.BlockSpec(memory_space=pltpu.VMEM)


def call(kernel, out_shape, in_specs, scratch=(), flops=0):
    return pl.pallas_call(
        kernel,
        out_shape=out_shape,
        in_specs=in_specs,
        out_specs=jax.tree.map(lambda _: VM, out_shape),
        scratch_shapes=list(scratch),
        cost_estimate=pl.CostEstimate(flops=flops, bytes_accessed=0, transcendentals=0),
        compiler_params=pltpu.CompilerParams(vmem_limit_bytes=VMEM_LIMIT),
    )


def whole(sp, tp, tokens, wk, wv, wd, decay_offset, fresh_question):
    rows, width = tokens.shape
    key_cols, value_cols = wk.shape[1], wv.shape[1]
    heads = key_cols // CUE_WIDTH
    cols = 2 * key_cols + value_cols
    log_length = math.log(rows * tp * sp)
    offset = decay_offset.reshape(1, key_cols)
    question = fresh_question.reshape(1, key_cols)
    sds = jax.ShapeDtypeStruct
    state_sds = sds((DV, key_cols), F32)
    total_sds = sds((1, key_cols), F32)

    late = rows // LATE_PARTS
    cuts = [(0, rows - late), (rows - late, rows)]
    far = {}
    for bit in range(1, tp // 2):
        for part, (lo, hi) in enumerate(cuts):
            far[bit, part] = lax.ppermute(tokens[lo:hi], "tp", swap(tp, 2 * bit))
    sibling = lax.ppermute(tokens, "tp", swap(tp, 1))

    s_near, l_near = call(
        functools.partial(near_kernel, log_length=log_length),
        (state_sds, total_sds),
        [VM] * 6,
        flops=4 * rows * width * cols,
    )(tokens, sibling, wk, wv, wd, offset)

    blocks, states, totals = [None], [s_near], [l_near]
    payload = None
    order = list(far)
    for n, (bit, part) in enumerate(order):
        a = far[bit, part]
        b = lax.ppermute(a, "tp", swap(tp, 1))
        flops = 4 * a.shape[0] * width * cols
        if n < len(order) - 1:
            s_a, s_b, l_a, l_b = call(
                functools.partial(early_kernel, log_length=log_length),
                (state_sds, state_sds, total_sds, total_sds),
                [VM] * 6,
                flops=flops,
            )(a, b, wk, wv, wd, offset)
            blocks += [(bit, part, True), (bit, part, False)]
            states += [s_a, s_b]
            totals += [l_a, l_b]
        else:
            payload = call(
                functools.partial(
                    late_kernel,
                    log_length=log_length,
                    blocks=tuple(blocks),
                    here=(bit, part),
                    parts=len(cuts),
                ),
                payload_sds(heads),
                [VM] * (6 + 2 * len(blocks)),
                flops=flops,
            )(a, b, wk, wv, wd, offset, *states, *totals)

    bits = [1 << n for n in range(sp.bit_length() - 1)]
    while len(bits) > 1:
        take = 2 if len(bits) > 2 else 1
        group, bits = bits[:take], bits[take:]
        others = [
            lax.ppermute(payload, "sp", swap(sp, sum(b for n, b in enumerate(group) if k >> n & 1)))
            for k in range(1, 2**take)
        ]
        payload, exact = call(
            functools.partial(merge_kernel, bits=tuple(group)),
            (payload_sds(heads), state_sds),
            [VM] * (2 + len(others)),
        )(question, payload, *others)
    other = lax.ppermute(payload, "sp", swap(sp, bits[0]))
    return call(
        functools.partial(final_kernel, bit=bits[0]),
        (sds((heads, CUE_WIDTH // sp, DV), BF16), sds((heads, DV), BF16)),
        [VM] * 4,
    )(question, payload, other, exact)


def solution(mesh):
    sp, tp = mesh.shape["sp"], mesh.shape["tp"]
    in_specs = (
        P(("sp", "tp"), None),
        P(None, "tp"),
        P(None, "tp"),
        P(None, "tp"),
        P("tp"),
        P("tp", None),
    )
    out_specs = (P("tp", "sp", None), P("tp", None))
    return jax.shard_map(
        functools.partial(whole, sp, tp),
        mesh=mesh,
        in_specs=in_specs,
        out_specs=out_specs,
        check_vma=False,
    )
```

time: 156 us -> 62 us (0.40)
  waiting for transfers between devices: 106 us -> 33 us
  blocking collectives: 20.5 us -> 0 us
  between operations: 14.1 us -> 0.75 us
  starting transfers between devices: 0.08 us -> 11.1 us
  matrix products: 10.3 us -> 0 us
  Pallas kernels: 0 us -> 9.51 us
  local copies, waits for them, and re-layouts: 2.13 us -> 7.41 us
  other arithmetic: 1.74 us -> 0 us
    psum x1 -> x0, waiting for transfers between devices: 67 us -> none  [per_device(): recall_grid = lax.psum(summands_list, 'sp')]
    all_gather x1 -> x0, waiting for transfers between devices: 38.8 us -> none  [per_device(): lax.all_gather(tokens, 'tp', axis=0, tiled=True)]
    ppermute x0 -> x9, waiting for transfers between devices: none -> 33 us  [the longest x2 24.5 us: whole(): far[bit, part] = lax.ppermute(tokens[lo:hi], 'tp', swap(tp, 2 * bit))]
    all_gather x1 -> x0, blocking collectives: 20.5 us -> none  [carried_in(): gathered = lax.all_gather(part, axis)]
    ppermute x0 -> x9, starting transfers between devices: none -> 11.1 us  [the longest x2 4.87 us: whole(): far[bit, part] = lax.ppermute(tokens[lo:hi], 'tp', swap(tp, 2 * bit))]
    dot_general x3 -> x0, matrix products: 10.3 us -> none  [the longest x1 8.32 us: per_device(): jnp.dot(lax.all_gather(tokens, 'tp', axis=0, tiled=True), combined, prefe...]
    pallas_call x0 -> x5, Pallas kernels: none -> 9.51 us  [the longest x1 3.4 us: whole(): call(functools.partial(near_kernel, log_length=log_length), (state_sds, t...]
    unnamed x6 -> x16, local copies, waits for them, and re-layouts: 0.02 us -> 5.02 us
  transfers between devices with their start and end apart: 2 -> 9, of which waited for: 2 -> 6; matrix products, arithmetic and copies ran while one was open for 0% -> 2% of each run, Pallas kernels for 0% -> 10%
where the time goes in v1:
time: 62 us; the launch traced here: 61.7 us
  waiting for transfers between devices  33 us (53%)
  starting transfers between devices  11.1 us (18%)
  Pallas kernels  9.51 us (15%)
  local copies, waits for them, and re-layouts  7.41 us (12%)
  between operations  0.75 us (1%)
    ppermute x2, waiting for transfers between devices, whole(): far[bit, part] = lax.ppermute(tokens[lo:hi], 'tp', swap(tp, 2 * bit))  24.5 us
    unnamed x16, local copies, waits for them, and re-layouts  5.02 us
    ppermute x3, waiting for transfers between devices, whole(): lax.ppermute(payload, 'sp', swap(sp, sum((b for n, b in enumerate(group)...  4.97 us
    ppermute x2, starting transfers between devices, whole(): far[bit, part] = lax.ppermute(tokens[lo:hi], 'tp', swap(tp, 2 * bit))  4.87 us
    ppermute x3, starting transfers between devices, whole(): lax.ppermute(payload, 'sp', swap(sp, sum((b for n, b in enumerate(group)...  3.55 us
    ppermute x1, waiting for transfers between devices, whole(): other = lax.ppermute(payload, 'sp', swap(sp, bits[0]))  3.46 us
    pallas_call x1, Pallas kernels, whole(): call(functools.partial(near_kernel, log_length=log_length), (state_sds, t...  3.4 us
    pallas_call x1, Pallas kernels, whole(): call(functools.partial(early_kernel, log_length=log_length), (state_sds,...  2.69 us
  transfers between devices with their start and end apart: 9, of which 6 were waited for; matrix products, arithmetic and copies ran while one was open for 2% of the time, Pallas kernels for 10%

profile of v1, /device:TPU:0, one launch (start us, length us, event | category | flops | bytes accessed | tf_op | source)
XLA Modules:
  0.0 61.7 jit_solution(15593946197330033332)
XLA Ops:
  0.6 0.0 copy-start.6
  0.6 1.3 %slice.7 = bf16[96,4096]{1,0:T(8,128)(2,1)S(1)} slice(bf16[128,4096]{1,0:T(8,128)(2,1)} %x0.1), slice={[0:96], [0:4096]} | slice | bytes 1572864 | tf_op jit(solution)/shard_map/slice | solution.py:280
  2.0 3.1 %collective-permute-start.3 = (bf16[96,4096]{1,0:T(8,128)(2,1)S(1)}, bf16[96,4096]{1,0:T(8,128)(2,1)S(1)}, u32[]{:S(2)}, u32[]{:S(2)}) collective-permute-start(bf16[96,4096]{1,0:T(8,128)(2,1)S(1)} %slice.7), channel_id=1, source_target_pairs={{0,2},{1,3},{2,0},{3,1},{4,6},{5,7},{6,4},{7,5},{8,10},{9,11},{10,... | collective-permute-start | bytes 2359304 | tf_op jit(solution)/shard_map/ppermute | solution.py:280
  5.0 0.0 collective-permute-start.2
  5.1 17.5 %collective-permute-done.3.xa = bf16[96,4096]{1,0:T(8,128)(2,1)S(1)} collective-permute-done((bf16[96,4096]{1,0:T(8,128)(2,1)S(1)}, bf16[96,4096]{1,0:T(8,128)(2,1)S(1)}, u32[]{:S(2)}, u32[]{:S(2)}) %collective-permute-start.3) | collective-permute-done | bytes 786464 | tf_op jit(solution)/shard_map/ppermute | solution.py:280
  22.6 0.0 collective-permute-start.4
  22.6 1.0 %slice.6 = bf16[32,4096]{1,0:T(8,128)(2,1)S(1)} slice(bf16[128,4096]{1,0:T(8,128)(2,1)} %x0.1), slice={[96:128], [0:4096]} | slice | bytes 524288 | tf_op jit(solution)/shard_map/slice | solution.py:280
  23.6 1.8 %collective-permute-start = (bf16[32,4096]{1,0:T(8,128)(2,1)S(1)}, bf16[32,4096]{1,0:T(8,128)(2,1)S(1)}, u32[]{:S(2)}, u32[]{:S(2)}) collective-permute-start(bf16[32,4096]{1,0:T(8,128)(2,1)S(1)} %slice.6), channel_id=1, source_target_pairs={{0,2},{1,3},{2,0},{3,1},{4,6},{5,7},{6,4},{7,5},{8,10},{9,11},{10,... | collective-permute-start | bytes 786440 | tf_op jit(solution)/shard_map/ppermute | solution.py:280
  25.4 7.0 %collective-permute-done.xa = bf16[32,4096]{1,0:T(8,128)(2,1)S(1)} collective-permute-done((bf16[32,4096]{1,0:T(8,128)(2,1)S(1)}, bf16[32,4096]{1,0:T(8,128)(2,1)S(1)}, u32[]{:S(2)}, u32[]{:S(2)}) %collective-permute-start) | collective-permute-done | bytes 262176 | tf_op jit(solution)/shard_map/ppermute | solution.py:280
  32.3 0.0 collective-permute-start.1
  32.4 0.0 collective-permute-done.2.x1
  32.4 0.0 copy-start
  32.4 2.2 %copy-done = bf16[4096,512]{1,0:T(8,128)(2,1)S(1)} copy-done((bf16[4096,512]{1,0:T(8,128)(2,1)S(1)}, bf16[4096,512]{1,0:T(8,128)(2,1)}, u32[]{:S(2)}) %copy-start) | copy-done | bytes 4194328
  34.6 1.6 %copy-done.3 = bf16[4096,256]{1,0:T(8,128)(2,1)S(1)} copy-done((bf16[4096,256]{1,0:T(8,128)(2,1)S(1)}, bf16[4096,256]{1,0:T(8,128)(2,1)}, u32[]{:S(2)}) %copy-start.3) | copy-done | bytes 2097176
  36.2 1.2 %copy-done.5 = bf16[128,4096]{1,0:T(8,128)(2,1)S(1)} copy-done((bf16[128,4096]{1,0:T(8,128)(2,1)S(1)}, bf16[128,4096]{1,0:T(8,128)(2,1)}, u32[]{:S(2)}) %copy-start.5) | copy-done | bytes 1048600
  37.4 3.4 %shard_map.77 = (f32[128,256]{1,0:T(8,128)S(1)}, f32[1,256]{1,0:T(1,128)S(1)}) custom-call(bf16[128,4096]{1,0:T(8,128)(2,1)S(1)} %copy-done.5, bf16[128,4096]{1,0:T(8,128)(2,1)S(1)} %collective-permute-done.2.x1, bf16[4096,256]{1,0:T(8,128)(2,1)S(1)} %copy-done.2, bf16[4096,512]{1,0:T(8,128)(2,1)S(1)} %copy-done, bf16[4096,256]{1,0:T(8,128)(2,1)S(1)} %copy-done.3, ...), custom_call_target="tpu_custom_call" | custom-call | flops 2147483648 | tf_op jit(solution)/shard_map/pallas_call | solution.py:283
  40.8 0.0 collective-permute-done.4.xb
  40.8 2.7 %shard_map.78 = (f32[128,256]{1,0:T(8,128)S(1)}, f32[128,256]{1,0:T(8,128)S(1)}, f32[1,256]{1,0:T(1,128)S(1)}, f32[1,256]{1,0:T(1,128)S(1)}) custom-call(bf16[96,4096]{1,0:T(8,128)(2,1)S(1)} %collective-permute-done.3.xa, bf16[96,4096]{1,0:T(8,128)(2,1)S(1)} %collective-permute-done.4.xb, bf16[4096,256]{1,0:T(8,128)(2,1)S(1)} %copy-done.2, ...), custom_call_target="tpu_custom_call" | custom-call | flops 1610612736 | tf_op jit(solution)/shard_map/pallas_call | solution.py:298
  43.5 0.0 collective-permute-done.1.xb
  43.5 0.0 copy-start.7
  43.5 2.1 %shard_map.79.refs_0_ = bf16[144,256]{1,0:T(8,128)(2,1)S(1)} custom-call(bf16[32,4096]{1,0:T(8,128)(2,1)S(1)} %collective-permute-done.xa, bf16[32,4096]{1,0:T(8,128)(2,1)S(1)} %collective-permute-done.1.xb, bf16[4096,256]{1,0:T(8,128)(2,1)S(1)} %copy-done.2, bf16[4096,512]{1,0:T(8,128)(2,1)S(1)} %copy-done.1, bf16[4096,256]{1,0:T(8,128)(2,1)S(1)} %copy-done.4, ...), custom_call_target="tpu_custom_call" | custom-call | flops 536870912 | tf_op jit(solution)/shard_map/pallas_call | solution.py:308
  45.6 1.8 %collective-permute-start.5 = (bf16[144,256]{1,0:T(8,128)(2,1)S(1)}, bf16[144,256]{1,0:T(8,128)(2,1)S(1)}, u32[]{:S(2)}, u32[]{:S(2)}) collective-permute-start(bf16[144,256]{1,0:T(8,128)(2,1)S(1)} %shard_map.79.refs_0_), channel_id=1, source_target_pairs={{0,4},{4,0},{8,12},{12,8},{16,20},{20,16},{24,28},{28,24},{1,5},{5... | collective-permute-start | bytes 221192 | tf_op jit(solution)/shard_map/ppermute | solution.py:326
  47.4 1.6 %collective-permute-start.6 = (bf16[144,256]{1,0:T(8,128)(2,1)S(1)}, bf16[144,256]{1,0:T(8,128)(2,1)S(1)}, u32[]{:S(2)}, u32[]{:S(2)}) collective-permute-start(bf16[144,256]{1,0:T(8,128)(2,1)S(1)} %shard_map.79.refs_0_), channel_id=1, source_target_pairs={{0,8},{4,12},{8,0},{12,4},{16,24},{20,28},{24,16},{28,20},{1,9},{5... | collective-permute-start | bytes 221192 | tf_op jit(solution)/shard_map/ppermute | solution.py:326
  49.0 0.2 collective-permute-start.7
  49.2 0.1 reshape.10.question
  49.3 1.1 %collective-permute-done.5.refs_1_ = bf16[144,256]{1,0:T(8,128)(2,1)S(1)} collective-permute-done((bf16[144,256]{1,0:T(8,128)(2,1)S(1)}, bf16[144,256]{1,0:T(8,128)(2,1)S(1)}, u32[]{:S(2)}, u32[]{:S(2)}) %collective-permute-start.5) | collective-permute-done | bytes 73760 | tf_op jit(solution)/shard_map/ppermute | solution.py:326
  50.4 1.7 %collective-permute-done.6.refs_2_ = bf16[144,256]{1,0:T(8,128)(2,1)S(1)} collective-permute-done((bf16[144,256]{1,0:T(8,128)(2,1)S(1)}, bf16[144,256]{1,0:T(8,128)(2,1)S(1)}, u32[]{:S(2)}, u32[]{:S(2)}) %collective-permute-start.6) | collective-permute-done | bytes 73760 | tf_op jit(solution)/shard_map/ppermute | solution.py:326
  52.1 2.1 %collective-permute-done.7.refs_3_ = bf16[144,256]{1,0:T(8,128)(2,1)S(1)} collective-permute-done((bf16[144,256]{1,0:T(8,128)(2,1)S(1)}, bf16[144,256]{1,0:T(8,128)(2,1)S(1)}, u32[]{:S(2)}, u32[]{:S(2)}) %collective-permute-start.7) | collective-permute-done | bytes 73760 | tf_op jit(solution)/shard_map/ppermute | solution.py:326
  54.3 0.3 shard_map.80
  54.6 2.6 %collective-permute-start.8 = (bf16[144,256]{1,0:T(8,128)(2,1)S(1)}, bf16[144,256]{1,0:T(8,128)(2,1)S(1)}, u32[]{:S(2)}, u32[]{:S(2)}) collective-permute-start(bf16[144,256]{1,0:T(8,128)(2,1)S(1)} %get-tuple-element.16.mine), channel_id=1, source_target_pairs={{0,16},{4,20},{8,24},{12,28},{16,0},{20,4},{24,8},{28,12},{1,17},{... | collective-permute-start | bytes 221192 | tf_op jit(solution)/shard_map/ppermute | solution.py:334
  57.2 3.5 %collective-permute-done.8.other = bf16[144,256]{1,0:T(8,128)(2,1)S(1)} collective-permute-done((bf16[144,256]{1,0:T(8,128)(2,1)S(1)}, bf16[144,256]{1,0:T(8,128)(2,1)S(1)}, u32[]{:S(2)}, u32[]{:S(2)}) %collective-permute-start.8) | collective-permute-done | bytes 73760 | tf_op jit(solution)/shard_map/ppermute | solution.py:334
  60.7 1.0 %shard_map.81 = (bf16[4,8,128]{2,1,0:T(8,128)(2,1)}, bf16[4,128]{1,0:T(4,128)(2,1)}) custom-call(bf16[1,256]{1,0:T(2,128)(2,1)S(1)} %reshape.10.question, bf16[144,256]{1,0:T(8,128)(2,1)S(1)} %get-tuple-element.16.mine, bf16[144,256]{1,0:T(8,128)(2,1)S(1)} %collective-permute-done.8.other, f32[128,256]{1,0:T(8,128)S(1)} %get-tuple-element.17.exact), custom_call_target="tpu_custom_call" | custom-call | tf_op jit(solution)/shard_map/pallas_call | solution.py:335
  (10 shorter events, 0.0 us)
Async XLA Ops:
  0.6 31.7 %copy-start.6 = (f32[256]{0:T(256)S(1)}, f32[256]{0:T(256)}, u32[]{:S(2)}) copy-start(f32[256]{0:T(256)} %param.10) | copy-start | bytes 3076
  0.6 31.7 %copy-start.2 = (bf16[4096,256]{1,0:T(8,128)(2,1)S(1)}, bf16[4096,256]{1,0:T(8,128)(2,1)}, u32[]{:S(2)}) copy-start(bf16[4096,256]{1,0:T(8,128)(2,1)} %wk.5) | copy-start | bytes 6291460
  2.0 20.6 %collective-permute-start.3 = (bf16[96,4096]{1,0:T(8,128)(2,1)S(1)}, bf16[96,4096]{1,0:T(8,128)(2,1)S(1)}, u32[]{:S(2)}, u32[]{:S(2)}) collective-permute-start(bf16[96,4096]{1,0:T(8,128)(2,1)S(1)} %slice.7), channel_id=1, source_target_pairs={{0,2},{1,3},{2,0},{3,1},{4,6},{5,7},{6,4},{7,5},{8,10},{9,11},{10,... | collective-permute-start | bytes 2359304 | tf_op jit(solution)/shard_map/ppermute | solution.py:280
  5.0 27.3 %collective-permute-start.2 = (bf16[128,4096]{1,0:T(8,128)(2,1)}, bf16[128,4096]{1,0:T(8,128)(2,1)S(1)}, u32[]{:S(2)}, u32[]{:S(2)}) collective-permute-start(bf16[128,4096]{1,0:T(8,128)(2,1)} %x0.1), channel_id=1, source_target_pairs={{0,1},{1,0},{2,3},{3,2},{4,5},{5,4},{6,7},{7,6},{8,9},{9,8},{10,11... | collective-permute-start | bytes 3145736 | tf_op jit(solution)/shard_map/ppermute | solution.py:281
  22.6 18.2 %collective-permute-start.4 = (bf16[96,4096]{1,0:T(8,128)(2,1)S(1)}, bf16[96,4096]{1,0:T(8,128)(2,1)S(1)}, u32[]{:S(2)}, u32[]{:S(2)}) collective-permute-start(bf16[96,4096]{1,0:T(8,128)(2,1)S(1)} %collective-permute-done.3.xa), channel_id=1, source_target_pairs={{0,1},{1,0},{2,3},{3,2},{4,5},{5,4},{6,7},{7,6},{8,9},{9,8},{10,11... | collective-permute-start | bytes 2359304 | tf_op jit(solution)/shard_map/ppermute | solution.py:295
  23.6 8.8 %collective-permute-start = (bf16[32,4096]{1,0:T(8,128)(2,1)S(1)}, bf16[32,4096]{1,0:T(8,128)(2,1)S(1)}, u32[]{:S(2)}, u32[]{:S(2)}) collective-permute-start(bf16[32,4096]{1,0:T(8,128)(2,1)S(1)} %slice.6), channel_id=1, source_target_pairs={{0,2},{1,3},{2,0},{3,1},{4,6},{5,7},{6,4},{7,5},{8,10},{9,11},{10,... | collective-permute-start | bytes 786440 | tf_op jit(solution)/shard_map/ppermute | solution.py:280
  32.3 11.2 %collective-permute-start.1 = (bf16[32,4096]{1,0:T(8,128)(2,1)S(1)}, bf16[32,4096]{1,0:T(8,128)(2,1)S(1)}, u32[]{:S(2)}, u32[]{:S(2)}) collective-permute-start(bf16[32,4096]{1,0:T(8,128)(2,1)S(1)} %collective-permute-done.xa), channel_id=1, source_target_pairs={{0,1},{1,0},{2,3},{3,2},{4,5},{5,4},{6,7},{7,6},{8,9},{9,8},{10,11... | collective-permute-start | bytes 786440 | tf_op jit(solution)/shard_map/ppermute | solution.py:295
  32.4 2.2 %copy-start = (bf16[4096,512]{1,0:T(8,128)(2,1)S(1)}, bf16[4096,512]{1,0:T(8,128)(2,1)}, u32[]{:S(2)}) copy-start(bf16[4096,512]{1,0:T(8,128)(2,1)} %wv.5) | copy-start | bytes 12582916
  34.6 1.6 %copy-start.3 = (bf16[4096,256]{1,0:T(8,128)(2,1)S(1)}, bf16[4096,256]{1,0:T(8,128)(2,1)}, u32[]{:S(2)}) copy-start(bf16[4096,256]{1,0:T(8,128)(2,1)} %wd.5) | copy-start | bytes 6291460
  36.2 1.2 %copy-start.5 = (bf16[128,4096]{1,0:T(8,128)(2,1)S(1)}, bf16[128,4096]{1,0:T(8,128)(2,1)}, u32[]{:S(2)}) copy-start(bf16[128,4096]{1,0:T(8,128)(2,1)} %x0.1) | copy-start | bytes 3145732
  37.4 3.4 %copy-start.1 = (bf16[4096,512]{1,0:T(8,128)(2,1)S(1)}, bf16[4096,512]{1,0:T(8,128)(2,1)}, u32[]{:S(2)}) copy-start(bf16[4096,512]{1,0:T(8,128)(2,1)} %wv.5) | copy-start | bytes 12582916
  37.4 3.4 %copy-start.4 = (bf16[4096,256]{1,0:T(8,128)(2,1)S(1)}, bf16[4096,256]{1,0:T(8,128)(2,1)}, u32[]{:S(2)}) copy-start(bf16[4096,256]{1,0:T(8,128)(2,1)} %wd.5) | copy-start | bytes 6291460
  43.5 5.7 %copy-start.7 = (bf16[4,64]{1,0:T(4,128)(2,1)S(1)}, bf16[4,64]{1,0:T(4,128)(2,1)}, u32[]{:S(2)}) copy-start(bf16[4,64]{1,0:T(4,128)(2,1)} %param.11) | copy-start | bytes 1540
  45.6 4.7 %collective-permute-start.5 = (bf16[144,256]{1,0:T(8,128)(2,1)S(1)}, bf16[144,256]{1,0:T(8,128)(2,1)S(1)}, u32[]{:S(2)}, u32[]{:S(2)}) collective-permute-start(bf16[144,256]{1,0:T(8,128)(2,1)S(1)} %shard_map.79.refs_0_), channel_id=1, source_target_pairs={{0,4},{4,0},{8,12},{12,8},{16,20},{20,16},{24,28},{28,24},{1,5},{5... | collective-permute-start | bytes 221192 | tf_op jit(solution)/shard_map/ppermute | solution.py:326
  47.4 4.7 %collective-permute-start.6 = (bf16[144,256]{1,0:T(8,128)(2,1)S(1)}, bf16[144,256]{1,0:T(8,128)(2,1)S(1)}, u32[]{:S(2)}, u32[]{:S(2)}) collective-permute-start(bf16[144,256]{1,0:T(8,128)(2,1)S(1)} %shard_map.79.refs_0_), channel_id=1, source_target_pairs={{0,8},{4,12},{8,0},{12,4},{16,24},{20,28},{24,16},{28,20},{1,9},{5... | collective-permute-start | bytes 221192 | tf_op jit(solution)/shard_map/ppermute | solution.py:326
  49.0 5.3 %collective-permute-start.7 = (bf16[144,256]{1,0:T(8,128)(2,1)S(1)}, bf16[144,256]{1,0:T(8,128)(2,1)S(1)}, u32[]{:S(2)}, u32[]{:S(2)}) collective-permute-start(bf16[144,256]{1,0:T(8,128)(2,1)S(1)} %shard_map.79.refs_0_), channel_id=1, source_target_pairs={{0,12},{4,8},{8,4},{12,0},{16,28},{20,24},{24,20},{28,16},{1,13},{... | collective-permute-start | bytes 221192 | tf_op jit(solution)/shard_map/ppermute | solution.py:326
  54.6 6.1 %collective-permute-start.8 = (bf16[144,256]{1,0:T(8,128)(2,1)S(1)}, bf16[144,256]{1,0:T(8,128)(2,1)S(1)}, u32[]{:S(2)}, u32[]{:S(2)}) collective-permute-start(bf16[144,256]{1,0:T(8,128)(2,1)S(1)} %get-tuple-element.16.mine), channel_id=1, source_target_pairs={{0,16},{4,20},{8,24},{12,28},{16,0},{20,4},{24,8},{28,12},{1,17},{... | collective-permute-start | bytes 221192 | tf_op jit(solution)/shard_map/ppermute | solution.py:334

commit v2 on v1

--- a/solution.py
+++ b/solution.py
@@ -12,7 +12,7 @@
 CUE_WIDTH = 64
 DV = 128
 DECAY_TAU = 16.0
-LATE_PARTS = 4
+ROW_PARTS = (1, 5, 2)
 VMEM_LIMIT = 24 * 1024 * 1024
 
 
@@ -34,14 +34,15 @@
     return keys, values, log_decay
 
 
-def later_within(log_decay, blocks):
+def later_within(log_decay, sizes):
     rows = log_decay.shape[0]
-    size = rows // blocks
     i = lax.broadcasted_iota(jnp.int32, (rows, rows), 0)
     j = lax.broadcasted_iota(jnp.int32, (rows, rows), 1)
     mask = j > i
-    for b in range(1, blocks):
-        mask = mask & ((i >= b * size) == (j >= b * size))
+    edge = 0
+    for size in sizes[:-1]:
+        edge += size
+        mask = mask & ((i >= edge) == (j >= edge))
     return jnp.dot(mask.astype(F32), log_decay, precision=EXACT, preferred_element_type=F32)
 
 
@@ -133,7 +134,7 @@
     rows = x0.shape[0]
     x = jnp.concatenate([x0[...], x1[...]], axis=0)
     keys, values, log_decay = project(x, wk, wv, wd, off[...], log_length)
-    after = later_within(log_decay, 2)
+    after = later_within(log_decay, [rows, rows])
     own = after[0:1] + log_decay[0:1]
     sib = after[rows : rows + 1] + log_decay[rows : rows + 1]
     own_tail = jnp.where(core == 0, sib, 0.0)
@@ -144,16 +145,20 @@
     l_out[...] = own + sib
 
 
-def early_kernel(xa, xb, wk, wv, wd, off, s_a, s_b, l_a, l_b, *, log_length):
-    rows = xa.shape[0]
-    x = jnp.concatenate([xa[...], xb[...]], axis=0)
+def early_kernel(*refs, log_length, blocks):
+    wk, wv, wd, off = refs[blocks : blocks + 4]
+    outs = refs[blocks + 4 :]
+    sizes = [ref.shape[0] for ref in refs[:blocks]]
+    x = jnp.concatenate([ref[...] for ref in refs[:blocks]], axis=0)
     keys, values, log_decay = project(x, wk, wv, wd, off[...], log_length)
-    after = later_within(log_decay, 2)
+    after = later_within(log_decay, sizes)
     weighted = weigh(keys, after)
-    s_a[...] = outer(values[:rows], [w[:rows] for w in weighted])
-    s_b[...] = outer(values[rows:], [w[rows:] for w in weighted])
-    l_a[...] = after[0:1] + log_decay[0:1]
-    l_b[...] = after[rows : rows + 1] + log_decay[rows : rows + 1]
+    lo = 0
+    for n, size in enumerate(sizes):
+        hi = lo + size
+        outs[n][...] = outer(values[lo:hi], [w[lo:hi] for w in weighted])
+        outs[blocks + n][...] = after[lo : lo + 1] + log_decay[lo : lo + 1]
+        lo = hi
 
 
 def late_kernel(xa, xb, wk, wv, wd, off, *refs, log_length, blocks, here, parts):
@@ -174,7 +179,7 @@
 
     x = jnp.concatenate([xa[...], xb[...]], axis=0)
     keys, values, log_decay = project(x, wk, wv, wd, off[...], log_length)
-    after = later_within(log_decay, 2)
+    after = later_within(log_decay, [rows, rows])
     own = [
         after[0:1] + log_decay[0:1],
         after[rows : rows + 1] + log_decay[rows : rows + 1],
@@ -272,8 +277,8 @@
     state_sds = sds((DV, key_cols), F32)
     total_sds = sds((1, key_cols), F32)
 
-    late = rows // LATE_PARTS
-    cuts = [(0, rows - late), (rows - late, rows)]
+    edges = [rows * sum(ROW_PARTS[:n]) // sum(ROW_PARTS) for n in range(len(ROW_PARTS) + 1)]
+    cuts = list(zip(edges[:-1], edges[1:]))
     far = {}
     for bit in range(1, tp // 2):
         for part, (lo, hi) in enumerate(cuts):
@@ -288,44 +293,44 @@
     )(tokens, sibling, wk, wv, wd, offset)
 
     blocks, states, totals = [None], [s_near], [l_near]
-    payload = None
-    order = list(far)
-    for n, (bit, part) in enumerate(order):
-        a = far[bit, part]
-        b = lax.ppermute(a, "tp", swap(tp, 1))
-        flops = 4 * a.shape[0] * width * cols
-        if n < len(order) - 1:
-            s_a, s_b, l_a, l_b = call(
-                functools.partial(early_kernel, log_length=log_length),
-                (state_sds, state_sds, total_sds, total_sds),
-                [VM] * 6,
-                flops=flops,
-            )(a, b, wk, wv, wd, offset)
-            blocks += [(bit, part, True), (bit, part, False)]
-            states += [s_a, s_b]
-            totals += [l_a, l_b]
-        else:
-            payload = call(
-                functools.partial(
-                    late_kernel,
-                    log_length=log_length,
-                    blocks=tuple(blocks),
-                    here=(bit, part),
-                    parts=len(cuts),
-                ),
-                payload_sds(heads),
-                [VM] * (6 + 2 * len(blocks)),
-                flops=flops,
-            )(a, b, wk, wv, wd, offset, *states, *totals)
+    pairs = {}
+    for bit, part in far:
+        pairs[bit, part] = (far[bit, part], lax.ppermute(far[bit, part], "tp", swap(tp, 1)))
+    last = (tp // 2 - 1, len(cuts) - 1)
+    for bit in range(1, tp // 2):
+        taken = [key for key in pairs if key[0] == bit and key != last]
+        inputs = [x for key in taken for x in pairs[key]]
+        count = len(inputs)
+        outs = call(
+            functools.partial(early_kernel, log_length=log_length, blocks=count),
+            (state_sds,) * count + (total_sds,) * count,
+            [VM] * (count + 4),
+            flops=2 * sum(x.shape[0] for x in inputs) * width * cols,
+        )(*inputs, wk, wv, wd, offset)
+        blocks += [key + (same,) for key in taken for same in (True, False)]
+        states += outs[:count]
+        totals += outs[count:]
+    payload = call(
+        functools.partial(
+            late_kernel,
+            log_length=log_length,
+            blocks=tuple(blocks),
+            here=last,
+            parts=len(cuts),
+        ),
+        payload_sds(heads),
+        [VM] * (6 + 2 * len(blocks)),
+        flops=4 * pairs[last][0].shape[0] * width * cols,
+    )(*pairs[last], wk, wv, wd, offset, *states, *totals)
 
     bits = [1 << n for n in range(sp.bit_length() - 1)]
     while len(bits) > 1:
         take = 2 if len(bits) > 2 else 1
         group, bits = bits[:take], bits[take:]
-        others = [
-            lax.ppermute(payload, "sp", swap(sp, sum(b for n, b in enumerate(group) if k >> n & 1)))
-            for k in range(1, 2**take)
-        ]
+        others = []
+        for k in range(1, 2**take):
+            far_bits = sum(b for n, b in enumerate(group) if k >> n & 1)
+            others.append(lax.ppermute(payload, "sp", swap(sp, far_bits)))
         payload, exact = call(
             functools.partial(merge_kernel, bits=tuple(group)),
             (payload_sds(heads), state_sds),

time: 62 us -> 62.5 us (level)
  waiting for transfers between devices: 33 us -> 31.6 us
  local copies, waits for them, and re-layouts: 7.41 us -> 8.27 us
  starting transfers between devices: 11.1 us -> 11.9 us
    ppermute x2 -> x3, waiting for transfers between devices: 24.5 us -> 23.2 us  [whole(): far[bit, part] = lax.ppermute(tokens[lo:hi], 'tp', swap(tp, 2 * bit))]
    slice x2 -> x3, local copies, waits for them, and re-layouts: 2.3 us -> 3.16 us  [whole(): far[bit, part] = lax.ppermute(tokens[lo:hi], 'tp', swap(tp, 2 * bit))]
    ppermute x5 -> x6, starting transfers between devices: 3.56 us -> 4.07 us  [the longest x3 3.55 us: whole(): others.append(lax.ppermute(payload, 'sp', swap(sp, far_bits)))]
    ppermute x2 -> x3, starting transfers between devices: 4.87 us -> 5.22 us  [whole(): far[bit, part] = lax.ppermute(tokens[lo:hi], 'tp', swap(tp, 2 * bit))]
    ppermute x5 -> x6, waiting for transfers between devices: 4.97 us -> 4.98 us  [the longest x3 4.97 us: whole(): others.append(lax.ppermute(payload, 'sp', swap(sp, far_bits)))]
  transfers between devices with their start and end apart: 9 -> 11, of which waited for: 6 -> 6; matrix products, arithmetic and copies ran while one was open for 2% -> 3% of each run, Pallas kernels for 10% -> 10%
where the time goes in v2:
time: 62.5 us; the launch traced here: 62.2 us
  waiting for transfers between devices  31.6 us (51%)
  starting transfers between devices  11.9 us (19%)
  Pallas kernels  9.63 us (15%)
  local copies, waits for them, and re-layouts  8.27 us (13%)
  between operations  0.76 us (1%)
    ppermute x3, waiting for transfers between devices, whole(): far[bit, part] = lax.ppermute(tokens[lo:hi], 'tp', swap(tp, 2 * bit))  23.2 us
    ppermute x3, starting transfers between devices, whole(): far[bit, part] = lax.ppermute(tokens[lo:hi], 'tp', swap(tp, 2 * bit))  5.22 us
    unnamed x16, local copies, waits for them, and re-layouts  5.02 us
    ppermute x3, waiting for transfers between devices, whole(): others.append(lax.ppermute(payload, 'sp', swap(sp, far_bits)))  4.97 us
    ppermute x3, starting transfers between devices, whole(): others.append(lax.ppermute(payload, 'sp', swap(sp, far_bits)))  3.55 us
    pallas_call x1, Pallas kernels, whole(): call(functools.partial(near_kernel, log_length=log_length), (state_sds, t...  3.4 us
    ppermute x1, waiting for transfers between devices, whole(): other = lax.ppermute(payload, 'sp', swap(sp, bits[0]))  3.4 us
    slice x3, local copies, waits for them, and re-layouts, whole(): far[bit, part] = lax.ppermute(tokens[lo:hi], 'tp', swap(tp, 2 * bit))  3.16 us
  transfers between devices with their start and end apart: 11, of which 6 were waited for; matrix products, arithmetic and copies ran while one was open for 3% of the time, Pallas kernels for 10%

profile of v2, /device:TPU:0, one launch (start us, length us, event | category | flops | bytes accessed | tf_op | source)
XLA Modules:
  0.0 62.2 jit_solution(14885793804397414369)
XLA Ops:
  0.6 1.3 %slice.11 = bf16[80,4096]{1,0:T(8,128)(2,1)S(1)} slice(bf16[128,4096]{1,0:T(8,128)(2,1)} %x0.1), slice={[16:96], [0:4096]} | slice | bytes 1310720 | tf_op jit(solution)/shard_map/slice | solution.py:285
  1.9 3.1 %collective-permute-start.5 = (bf16[80,4096]{1,0:T(8,128)(2,1)S(1)}, bf16[80,4096]{1,0:T(8,128)(2,1)S(1)}, u32[]{:S(2)}, u32[]{:S(2)}) collective-permute-start(bf16[80,4096]{1,0:T(8,128)(2,1)S(1)} %slice.11), channel_id=1, source_target_pairs={{0,2},{1,3},{2,0},{3,1},{4,6},{5,7},{6,4},{7,5},{8,10},{9,11},{10,... | collective-permute-start | bytes 1966088 | tf_op jit(solution)/shard_map/ppermute | solution.py:285
  5.0 14.7 %collective-permute-done.5.refs_2_ = bf16[80,4096]{1,0:T(8,128)(2,1)S(1)} collective-permute-done((bf16[80,4096]{1,0:T(8,128)(2,1)S(1)}, bf16[80,4096]{1,0:T(8,128)(2,1)S(1)}, u32[]{:S(2)}, u32[]{:S(2)}) %collective-permute-start.5) | collective-permute-done | bytes 655392 | tf_op jit(solution)/shard_map/ppermute | solution.py:285
  19.7 0.0 collective-permute-start.6
  19.7 1.0 %slice.9 = bf16[32,4096]{1,0:T(8,128)(2,1)S(1)} slice(bf16[128,4096]{1,0:T(8,128)(2,1)} %x0.1), slice={[96:128], [0:4096]} | slice | bytes 524288 | tf_op jit(solution)/shard_map/slice | solution.py:285
  20.7 1.8 %collective-permute-start = (bf16[32,4096]{1,0:T(8,128)(2,1)S(1)}, bf16[32,4096]{1,0:T(8,128)(2,1)S(1)}, u32[]{:S(2)}, u32[]{:S(2)}) collective-permute-start(bf16[32,4096]{1,0:T(8,128)(2,1)S(1)} %slice.9), channel_id=1, source_target_pairs={{0,2},{1,3},{2,0},{3,1},{4,6},{5,7},{6,4},{7,5},{8,10},{9,11},{10,... | collective-permute-start | bytes 786440 | tf_op jit(solution)/shard_map/ppermute | solution.py:285
  22.5 0.9 %slice.10 = bf16[16,4096]{1,0:T(8,128)(2,1)S(1)} slice(bf16[128,4096]{1,0:T(8,128)(2,1)} %x0.1), slice={[0:16], [0:4096]} | slice | bytes 262144 | tf_op jit(solution)/shard_map/slice | solution.py:285
  23.4 0.4 collective-permute-start.3
  23.8 8.5 %collective-permute-done.3.refs_0_ = bf16[16,4096]{1,0:T(8,128)(2,1)S(1)} collective-permute-done((bf16[16,4096]{1,0:T(8,128)(2,1)S(1)}, bf16[16,4096]{1,0:T(8,128)(2,1)S(1)}, u32[]{:S(2)}, u32[]{:S(2)}) %collective-permute-start.3) | collective-permute-done | bytes 131104 | tf_op jit(solution)/shard_map/ppermute | solution.py:285
  32.3 0.0 collective-permute-start.4
  32.3 0.5 collective-permute-start.1
  32.8 0.0 copy-start
  32.8 2.2 %copy-done = bf16[4096,512]{1,0:T(8,128)(2,1)S(1)} copy-done((bf16[4096,512]{1,0:T(8,128)(2,1)S(1)}, bf16[4096,512]{1,0:T(8,128)(2,1)}, u32[]{:S(2)}) %copy-start) | copy-done | bytes 4194328
  35.0 1.6 %copy-done.3 = bf16[4096,256]{1,0:T(8,128)(2,1)S(1)} copy-done((bf16[4096,256]{1,0:T(8,128)(2,1)S(1)}, bf16[4096,256]{1,0:T(8,128)(2,1)}, u32[]{:S(2)}) %copy-start.3) | copy-done | bytes 2097176
  36.6 1.2 %copy-done.5 = bf16[128,4096]{1,0:T(8,128)(2,1)S(1)} copy-done((bf16[128,4096]{1,0:T(8,128)(2,1)S(1)}, bf16[128,4096]{1,0:T(8,128)(2,1)}, u32[]{:S(2)}) %copy-start.5) | copy-done | bytes 1048600
  37.8 3.4 %shard_map.77 = (f32[128,256]{1,0:T(8,128)S(1)}, f32[1,256]{1,0:T(1,128)S(1)}) custom-call(bf16[128,4096]{1,0:T(8,128)(2,1)S(1)} %copy-done.5, bf16[128,4096]{1,0:T(8,128)(2,1)S(1)} %collective-permute-done.2.x1, bf16[4096,256]{1,0:T(8,128)(2,1)S(1)} %copy-done.2, bf16[4096,512]{1,0:T(8,128)(2,1)S(1)} %copy-done, bf16[4096,256]{1,0:T(8,128)(2,1)S(1)} %copy-done.3, ...), custom_call_target="tpu_custom_call" | custom-call | flops 2147483648 | tf_op jit(solution)/shard_map/pallas_call | solution.py:288
  41.2 0.0 collective-permute-done.4.refs_1_
  41.3 2.8 %shard_map.78 = (f32[128,256]{1,0:T(8,128)S(1)}, f32[128,256]{1,0:T(8,128)S(1)}, f32[128,256]{1,0:T(8,128)S(1)}, f32[128,256]{1,0:T(8,128)S(1)}, f32[1,256]{1,0:...) custom-call(bf16[16,4096]{1,0:T(8,128)(2,1)S(1)} %collective-permute-done.3.refs_0_, ...), custom_call_target="tpu_custom_call" | custom-call | flops 1610612736 | tf_op jit(solution)/shard_map/pallas_call | solution.py:304
  44.1 0.0 collective-permute-done.1.xb
  44.1 0.0 copy-start.7
  44.1 2.1 %shard_map.79.refs_0_ = bf16[144,256]{1,0:T(8,128)(2,1)S(1)} custom-call(bf16[32,4096]{1,0:T(8,128)(2,1)S(1)} %collective-permute-done.xa, bf16[32,4096]{1,0:T(8,128)(2,1)S(1)} %collective-permute-done.1.xb, bf16[4096,256]{1,0:T(8,128)(2,1)S(1)} %copy-done.2, bf16[4096,512]{1,0:T(8,128)(2,1)S(1)} %copy-done.1, bf16[4096,256]{1,0:T(8,128)(2,1)S(1)} %copy-done.4, ...), custom_call_target="tpu_custom_call" | custom-call | flops 536870912 | tf_op jit(solution)/shard_map/pallas_call | solution.py:313
  46.2 1.8 %collective-permute-start.7 = (bf16[144,256]{1,0:T(8,128)(2,1)S(1)}, bf16[144,256]{1,0:T(8,128)(2,1)S(1)}, u32[]{:S(2)}, u32[]{:S(2)}) collective-permute-start(bf16[144,256]{1,0:T(8,128)(2,1)S(1)} %shard_map.79.refs_0_), channel_id=1, source_target_pairs={{0,4},{4,0},{8,12},{12,8},{16,20},{20,16},{24,28},{28,24},{1,5},{5... | collective-permute-start | bytes 221192 | tf_op jit(solution)/shard_map/ppermute | solution.py:333
  48.0 1.6 %collective-permute-start.8 = (bf16[144,256]{1,0:T(8,128)(2,1)S(1)}, bf16[144,256]{1,0:T(8,128)(2,1)S(1)}, u32[]{:S(2)}, u32[]{:S(2)}) collective-permute-start(bf16[144,256]{1,0:T(8,128)(2,1)S(1)} %shard_map.79.refs_0_), channel_id=1, source_target_pairs={{0,8},{4,12},{8,0},{12,4},{16,24},{20,28},{24,16},{28,20},{1,9},{5... | collective-permute-start | bytes 221192 | tf_op jit(solution)/shard_map/ppermute | solution.py:333
  49.6 0.2 collective-permute-start.9
  49.8 0.1 reshape.10.question
  49.9 0.8 %collective-permute-done.7.refs_1_ = bf16[144,256]{1,0:T(8,128)(2,1)S(1)} collective-permute-done((bf16[144,256]{1,0:T(8,128)(2,1)S(1)}, bf16[144,256]{1,0:T(8,128)(2,1)S(1)}, u32[]{:S(2)}, u32[]{:S(2)}) %collective-permute-start.7) | collective-permute-done | bytes 73760 | tf_op jit(solution)/shard_map/ppermute | solution.py:333
  50.7 2.5 %collective-permute-done.8.refs_2_ = bf16[144,256]{1,0:T(8,128)(2,1)S(1)} collective-permute-done((bf16[144,256]{1,0:T(8,128)(2,1)S(1)}, bf16[144,256]{1,0:T(8,128)(2,1)S(1)}, u32[]{:S(2)}, u32[]{:S(2)}) %collective-permute-start.8) | collective-permute-done | bytes 73760 | tf_op jit(solution)/shard_map/ppermute | solution.py:333
  53.1 1.7 %collective-permute-done.9.refs_3_ = bf16[144,256]{1,0:T(8,128)(2,1)S(1)} collective-permute-done((bf16[144,256]{1,0:T(8,128)(2,1)S(1)}, bf16[144,256]{1,0:T(8,128)(2,1)S(1)}, u32[]{:S(2)}, u32[]{:S(2)}) %collective-permute-start.9) | collective-permute-done | bytes 73760 | tf_op jit(solution)/shard_map/ppermute | solution.py:333
  54.8 0.3 shard_map.80
  55.2 2.7 %collective-permute-start.10 = (bf16[144,256]{1,0:T(8,128)(2,1)S(1)}, bf16[144,256]{1,0:T(8,128)(2,1)S(1)}, u32[]{:S(2)}, u32[]{:S(2)}) collective-permute-start(bf16[144,256]{1,0:T(8,128)(2,1)S(1)} %get-tuple-element.24.mine), channel_id=1, source_target_pairs={{0,16},{4,20},{8,24},{12,28},{16,0},{20,4},{24,8},{28,12},{1,17},{... | collective-permute-start | bytes 221192 | tf_op jit(solution)/shard_map/ppermute | solution.py:339
  57.8 3.4 %collective-permute-done.10.other = bf16[144,256]{1,0:T(8,128)(2,1)S(1)} collective-permute-done((bf16[144,256]{1,0:T(8,128)(2,1)S(1)}, bf16[144,256]{1,0:T(8,128)(2,1)S(1)}, u32[]{:S(2)}, u32[]{:S(2)}) %collective-permute-start.10) | collective-permute-done | bytes 73760 | tf_op jit(solution)/shard_map/ppermute | solution.py:339
  61.2 1.0 %shard_map.81 = (bf16[4,8,128]{2,1,0:T(8,128)(2,1)}, bf16[4,128]{1,0:T(4,128)(2,1)}) custom-call(bf16[1,256]{1,0:T(2,128)(2,1)S(1)} %reshape.10.question, bf16[144,256]{1,0:T(8,128)(2,1)S(1)} %get-tuple-element.24.mine, bf16[144,256]{1,0:T(8,128)(2,1)S(1)} %collective-permute-done.10.other, f32[128,256]{1,0:T(8,128)S(1)} %get-tuple-element.25.exact), custom_call_target="tpu_custom_call" | custom-call | tf_op jit(solution)/shard_map/pallas_call | solution.py:340
  (15 shorter events, 0.0 us)
Async XLA Ops:
  0.6 32.2 %copy-start.6 = (f32[256]{0:T(256)S(1)}, f32[256]{0:T(256)}, u32[]{:S(2)}) copy-start(f32[256]{0:T(256)} %param.10) | copy-start | bytes 3076
  0.6 32.2 %copy-start.2 = (bf16[4096,256]{1,0:T(8,128)(2,1)S(1)}, bf16[4096,256]{1,0:T(8,128)(2,1)}, u32[]{:S(2)}) copy-start(bf16[4096,256]{1,0:T(8,128)(2,1)} %wk.3) | copy-start | bytes 6291460
  1.9 17.8 %collective-permute-start.5 = (bf16[80,4096]{1,0:T(8,128)(2,1)S(1)}, bf16[80,4096]{1,0:T(8,128)(2,1)S(1)}, u32[]{:S(2)}, u32[]{:S(2)}) collective-permute-start(bf16[80,4096]{1,0:T(8,128)(2,1)S(1)} %slice.11), channel_id=1, source_target_pairs={{0,2},{1,3},{2,0},{3,1},{4,6},{5,7},{6,4},{7,5},{8,10},{9,11},{10,... | collective-permute-start | bytes 1966088 | tf_op jit(solution)/shard_map/ppermute | solution.py:285
  5.0 27.8 %collective-permute-start.2 = (bf16[128,4096]{1,0:T(8,128)(2,1)}, bf16[128,4096]{1,0:T(8,128)(2,1)S(1)}, u32[]{:S(2)}, u32[]{:S(2)}) collective-permute-start(bf16[128,4096]{1,0:T(8,128)(2,1)} %x0.1), channel_id=1, source_target_pairs={{0,1},{1,0},{2,3},{3,2},{4,5},{5,4},{6,7},{7,6},{8,9},{9,8},{10,11... | collective-permute-start | bytes 3145736 | tf_op jit(solution)/shard_map/ppermute | solution.py:286
  19.7 21.5 %collective-permute-start.6 = (bf16[80,4096]{1,0:T(8,128)(2,1)S(1)}, bf16[80,4096]{1,0:T(8,128)(2,1)S(1)}, u32[]{:S(2)}, u32[]{:S(2)}) collective-permute-start(bf16[80,4096]{1,0:T(8,128)(2,1)S(1)} %collective-permute-done.5.refs_2_), channel_id=1, source_target_pairs={{0,1},{1,0},{2,3},{3,2},{4,5},{5,4},{6,7},{7,6},{8,9},{9,8},{10,11... | collective-permute-start | bytes 1966088 | tf_op jit(solution)/shard_map/ppermute | solution.py:298
  20.7 11.6 %collective-permute-start = (bf16[32,4096]{1,0:T(8,128)(2,1)S(1)}, bf16[32,4096]{1,0:T(8,128)(2,1)S(1)}, u32[]{:S(2)}, u32[]{:S(2)}) collective-permute-start(bf16[32,4096]{1,0:T(8,128)(2,1)S(1)} %slice.9), channel_id=1, source_target_pairs={{0,2},{1,3},{2,0},{3,1},{4,6},{5,7},{6,4},{7,5},{8,10},{9,11},{10,... | collective-permute-start | bytes 786440 | tf_op jit(solution)/shard_map/ppermute | solution.py:285
  23.4 8.9 %collective-permute-start.3 = (bf16[16,4096]{1,0:T(8,128)(2,1)S(1)}, bf16[16,4096]{1,0:T(8,128)(2,1)S(1)}, u32[]{:S(2)}, u32[]{:S(2)}) collective-permute-start(bf16[16,4096]{1,0:T(8,128)(2,1)S(1)} %slice.10), channel_id=1, source_target_pairs={{0,2},{1,3},{2,0},{3,1},{4,6},{5,7},{6,4},{7,5},{8,10},{9,11},{10,... | collective-permute-start | bytes 393224 | tf_op jit(solution)/shard_map/ppermute | solution.py:285
  32.3 9.0 %collective-permute-start.4 = (bf16[16,4096]{1,0:T(8,128)(2,1)S(1)}, bf16[16,4096]{1,0:T(8,128)(2,1)S(1)}, u32[]{:S(2)}, u32[]{:S(2)}) collective-permute-start(bf16[16,4096]{1,0:T(8,128)(2,1)S(1)} %collective-permute-done.3.refs_0_), channel_id=1, source_target_pairs={{0,1},{1,0},{2,3},{3,2},{4,5},{5,4},{6,7},{7,6},{8,9},{9,8},{10,11... | collective-permute-start | bytes 393224 | tf_op jit(solution)/shard_map/ppermute | solution.py:298
  32.3 11.8 %collective-permute-start.1 = (bf16[32,4096]{1,0:T(8,128)(2,1)S(1)}, bf16[32,4096]{1,0:T(8,128)(2,1)S(1)}, u32[]{:S(2)}, u32[]{:S(2)}) collective-permute-start(bf16[32,4096]{1,0:T(8,128)(2,1)S(1)} %collective-permute-done.xa), channel_id=1, source_target_pairs={{0,1},{1,0},{2,3},{3,2},{4,5},{5,4},{6,7},{7,6},{8,9},{9,8},{10,11... | collective-permute-start | bytes 786440 | tf_op jit(solution)/shard_map/ppermute | solution.py:298
  32.8 2.2 %copy-start = (bf16[4096,512]{1,0:T(8,128)(2,1)S(1)}, bf16[4096,512]{1,0:T(8,128)(2,1)}, u32[]{:S(2)}) copy-start(bf16[4096,512]{1,0:T(8,128)(2,1)} %wv.3) | copy-start | bytes 12582916
  35.0 1.6 %copy-start.3 = (bf16[4096,256]{1,0:T(8,128)(2,1)S(1)}, bf16[4096,256]{1,0:T(8,128)(2,1)}, u32[]{:S(2)}) copy-start(bf16[4096,256]{1,0:T(8,128)(2,1)} %wd.3) | copy-start | bytes 6291460
  36.6 1.2 %copy-start.5 = (bf16[128,4096]{1,0:T(8,128)(2,1)S(1)}, bf16[128,4096]{1,0:T(8,128)(2,1)}, u32[]{:S(2)}) copy-start(bf16[128,4096]{1,0:T(8,128)(2,1)} %x0.1) | copy-start | bytes 3145732
  37.8 3.4 %copy-start.1 = (bf16[4096,512]{1,0:T(8,128)(2,1)S(1)}, bf16[4096,512]{1,0:T(8,128)(2,1)}, u32[]{:S(2)}) copy-start(bf16[4096,512]{1,0:T(8,128)(2,1)} %wv.3) | copy-start | bytes 12582916
  37.8 3.4 %copy-start.4 = (bf16[4096,256]{1,0:T(8,128)(2,1)S(1)}, bf16[4096,256]{1,0:T(8,128)(2,1)}, u32[]{:S(2)}) copy-start(bf16[4096,256]{1,0:T(8,128)(2,1)} %wd.3) | copy-start | bytes 6291460
  44.1 5.7 %copy-start.7 = (bf16[4,64]{1,0:T(4,128)(2,1)S(1)}, bf16[4,64]{1,0:T(4,128)(2,1)}, u32[]{:S(2)}) copy-start(bf16[4,64]{1,0:T(4,128)(2,1)} %param.11) | copy-start | bytes 1540
  46.2 4.4 %collective-permute-start.7 = (bf16[144,256]{1,0:T(8,128)(2,1)S(1)}, bf16[144,256]{1,0:T(8,128)(2,1)S(1)}, u32[]{:S(2)}, u32[]{:S(2)}) collective-permute-start(bf16[144,256]{1,0:T(8,128)(2,1)S(1)} %shard_map.79.refs_0_), channel_id=1, source_target_pairs={{0,4},{4,0},{8,12},{12,8},{16,20},{20,16},{24,28},{28,24},{1,5},{5... | collective-permute-start | bytes 221192 | tf_op jit(solution)/shard_map/ppermute | solution.py:333
  48.0 5.1 %collective-permute-start.8 = (bf16[144,256]{1,0:T(8,128)(2,1)S(1)}, bf16[144,256]{1,0:T(8,128)(2,1)S(1)}, u32[]{:S(2)}, u32[]{:S(2)}) collective-permute-start(bf16[144,256]{1,0:T(8,128)(2,1)S(1)} %shard_map.79.refs_0_), channel_id=1, source_target_pairs={{0,8},{4,12},{8,0},{12,4},{16,24},{20,28},{24,16},{28,20},{1,9},{5... | collective-permute-start | bytes 221192 | tf_op jit(solution)/shard_map/ppermute | solution.py:333
  49.6 5.3 %collective-permute-start.9 = (bf16[144,256]{1,0:T(8,128)(2,1)S(1)}, bf16[144,256]{1,0:T(8,128)(2,1)S(1)}, u32[]{:S(2)}, u32[]{:S(2)}) collective-permute-start(bf16[144,256]{1,0:T(8,128)(2,1)S(1)} %shard_map.79.refs_0_), channel_id=1, source_target_pairs={{0,12},{4,8},{8,4},{12,0},{16,28},{20,24},{24,20},{28,16},{1,13},{... | collective-permute-start | bytes 221192 | tf_op jit(solution)/shard_map/ppermute | solution.py:333
  55.2 6.1 %collective-permute-start.10 = (bf16[144,256]{1,0:T(8,128)(2,1)S(1)}, bf16[144,256]{1,0:T(8,128)(2,1)S(1)}, u32[]{:S(2)}, u32[]{:S(2)}) collective-permute-start(bf16[144,256]{1,0:T(8,128)(2,1)S(1)} %get-tuple-element.24.mine), channel_id=1, source_target_pairs={{0,16},{4,20},{8,24},{12,28},{16,0},{20,4},{24,8},{28,12},{1,17},{... | collective-permute-start | bytes 221192 | tf_op jit(solution)/shard_map/ppermute | solution.py:339

commit v3 on v2

--- a/solution.py
+++ b/solution.py
@@ -12,8 +12,8 @@
 CUE_WIDTH = 64
 DV = 128
 DECAY_TAU = 16.0
-ROW_PARTS = (1, 5, 2)
-VMEM_LIMIT = 24 * 1024 * 1024
+ROW_PARTS = (3, 8, 5)
+VMEM_LIMIT = 8 * 1024 * 1024
 
 
 F32 = jnp.float32
@@ -116,17 +116,33 @@
     return parts[0] + parts[1] + parts[2]
 
 
-def asking(question, rows):
-    row = lax.broadcasted_iota(jnp.int32, (rows, question.shape[1]), 0)
-    lane = lax.broadcasted_iota(jnp.int32, (rows, question.shape[1]), 1)
-    asked = question[...].astype(F32) * CUE_WIDTH ** (-0.5)
-    return jnp.where(lax.div(lane, CUE_WIDTH) == row, asked, 0.0)
+def ask_kernel(question, out):
+    row = lax.broadcasted_iota(jnp.int32, out.shape, 0)
+    lane = lax.broadcasted_iota(jnp.int32, out.shape, 1)
+    heads = question.shape[0]
+    asked = jnp.concatenate([question[...].astype(F32)] * heads, axis=1) * CUE_WIDTH ** (-0.5)
+    if out.shape[0] > heads:
+        spare = jnp.zeros((out.shape[0] - heads, out.shape[1]), F32)
+        asked = jnp.concatenate([asked, spare], axis=0)
+    out[...] = jnp.where(lax.div(lane, CUE_WIDTH) == row, asked, 0.0)
 
 
 def against(left, state):
     return lax.dot_general(
         left, state, (((1,), (1,)), ((), ())), precision=EXACT, preferred_element_type=F32
     )
+
+
+def cut_kernel(tokens, *refs, cuts):
+    sems = refs[-1]
+    copies = [
+        pltpu.make_async_copy(tokens.at[lo:hi, :], out, sems.at[n])
+        for n, ((lo, hi), out) in enumerate(zip(cuts, refs))
+    ]
+    for copy in copies:
+        copy.start()
+    for copy in copies:
+        copy.wait()
 
 
 def near_kernel(x0, x1, wk, wv, wd, off, s_out, l_out, *, log_length):
@@ -205,10 +221,10 @@
     pack(out, state, total)
 
 
-def merge_kernel(question, *refs, bits):
+def merge_kernel(asked, *refs, bits):
     count = 2 ** len(bits)
     out, exact = refs[count:]
-    key_cols = question.shape[1]
+    key_cols = asked.shape[1]
     parts = [unpack(ref, key_cols)[:2] for ref in refs[:count]]
     for n, bit in enumerate(bits):
         turned = lax.bitwise_and(lax.axis_index("sp"), bit) != 0
@@ -222,12 +238,12 @@
         total = total + t
     exact[...] = state
     heads = key_cols // CUE_WIDTH
-    pack(out, state, total, against(asking(question, 8), state)[:heads])
-
-
-def final_kernel(question, mine, other, exact, cache, read, *, bit):
+    pack(out, state, total, against(asked[...], state)[:heads])
+
+
+def final_kernel(asked, mine, other, exact, cache, read, *, bit):
     heads, kept, _ = cache.shape
-    key_cols = question.shape[1]
+    key_cols = asked.shape[1]
     earlier = lax.bitwise_and(lax.axis_index("sp"), bit) == 0
     s_m, l_m, tail_m = unpack(mine, key_cols)
     s_o, l_o, tail_o = unpack(other, key_cols)
@@ -244,7 +260,7 @@
     result = against(chosen, state)
     for h in range(heads):
         cache[h] = result[h * kept : (h + 1) * kept].astype(BF16)
-    heard = against(asking(question, 8), first)[:heads]
+    heard = against(asked[...], first)[:heads]
     heard = heard + heard_of(jnp.where(earlier, tail_o, tail_m), heads)
     mean = jnp.mean(heard * heard, axis=-1, keepdims=True)
     read[...] = (heard * lax.rsqrt(mean + 1.0)).astype(BF16)
@@ -272,17 +288,25 @@
     cols = 2 * key_cols + value_cols
     log_length = math.log(rows * tp * sp)
     offset = decay_offset.reshape(1, key_cols)
-    question = fresh_question.reshape(1, key_cols)
     sds = jax.ShapeDtypeStruct
     state_sds = sds((DV, key_cols), F32)
     total_sds = sds((1, key_cols), F32)
 
     edges = [rows * sum(ROW_PARTS[:n]) // sum(ROW_PARTS) for n in range(len(ROW_PARTS) + 1)]
     cuts = list(zip(edges[:-1], edges[1:]))
+    held = pltpu.with_memory_space_constraint(tokens, pltpu.HBM)
+    pieces = []
+    for some in (cuts[:1], cuts[1:]):
+        pieces += call(
+            functools.partial(cut_kernel, cuts=tuple(some)),
+            tuple(pltpu.VMEM((hi - lo, width), BF16) for lo, hi in some),
+            [pl.BlockSpec(memory_space=pltpu.HBM)],
+            [pltpu.SemaphoreType.DMA((len(some),))],
+        )(held)
     far = {}
     for bit in range(1, tp // 2):
-        for part, (lo, hi) in enumerate(cuts):
-            far[bit, part] = lax.ppermute(tokens[lo:hi], "tp", swap(tp, 2 * bit))
+        for part, piece in enumerate(pieces):
+            far[bit, part] = lax.ppermute(piece, "tp", swap(tp, 2 * bit))
     sibling = lax.ppermute(tokens, "tp", swap(tp, 1))
 
     s_near, l_near = call(
@@ -291,6 +315,8 @@
         [VM] * 6,
         flops=4 * rows * width * cols,
     )(tokens, sibling, wk, wv, wd, offset)
+
+    asked = call(ask_kernel, sds((heads + -heads % 8, key_cols), F32), [VM])(fresh_question)
 
     blocks, states, totals = [None], [s_near], [l_near]
     pairs = {}
@@ -335,13 +361,13 @@
             functools.partial(merge_kernel, bits=tuple(group)),
             (payload_sds(heads), state_sds),
             [VM] * (2 + len(others)),
-        )(question, payload, *others)
+        )(asked, payload, *others)
     other = lax.ppermute(payload, "sp", swap(sp, bits[0]))
     return call(
         functools.partial(final_kernel, bit=bits[0]),
         (sds((heads, CUE_WIDTH // sp, DV), BF16), sds((heads, DV), BF16)),
         [VM] * 4,
-    )(question, payload, other, exact)
+    )(asked, payload, other, exact)
 
 
 def solution(mesh):

time: 62.5 us -> 61.1 us (0.978)
  local copies, waits for them, and re-layouts: 8.27 us -> 4.17 us
  Pallas kernels: 9.63 us -> 11.9 us
  waiting for transfers between devices: 31.6 us -> 32.7 us
    slice x3 -> x0, local copies, waits for them, and re-layouts: 3.16 us -> none  [whole(): far[bit, part] = lax.ppermute(tokens[lo:hi], 'tp', swap(tp, 2 * bit))]
    pallas_call x0 -> x3, Pallas kernels: none -> 2.31 us  [the longest x2 2.24 us: whole(): call(functools.partial(cut_kernel, cuts=tuple(some)), tuple((pltpu.VMEM((...]
    ppermute x3, waiting for transfers between devices: 23.2 us -> 24.2 us  [whole(): far[bit, part] = lax.ppermute(piece, 'tp', swap(tp, 2 * bit))]
    unnamed x16, local copies, waits for them, and re-layouts: 5.02 us -> 4.17 us
  transfers between devices with their start and end apart: 11 -> 11, of which waited for: 6 -> 7; matrix products, arithmetic and copies ran while one was open for 3% -> 0% of each run, Pallas kernels for 10% -> 12%
where the time goes in v3:
time: 61.1 us; the launch traced here: 60.9 us
  waiting for transfers between devices  32.7 us (54%)
  Pallas kernels  11.9 us (19%)
  starting transfers between devices  11.4 us (19%)
  local copies, waits for them, and re-layouts  4.17 us (7%)
  between operations  0.76 us (1%)
    ppermute x3, waiting for transfers between devices, whole(): far[bit, part] = lax.ppermute(piece, 'tp', swap(tp, 2 * bit))  24.2 us
    ppermute x3, starting transfers between devices, whole(): far[bit, part] = lax.ppermute(piece, 'tp', swap(tp, 2 * bit))  5.15 us
    ppermute x3, waiting for transfers between devices, whole(): others.append(lax.ppermute(payload, 'sp', swap(sp, far_bits)))  4.98 us
    unnamed x16, local copies, waits for them, and re-layouts  4.17 us
    ppermute x3, starting transfers between devices, whole(): others.append(lax.ppermute(payload, 'sp', swap(sp, far_bits)))  3.55 us
    pallas_call x1, Pallas kernels, whole(): call(functools.partial(near_kernel, log_length=log_length), (state_sds, t...  3.46 us
    ppermute x1, waiting for transfers between devices, whole(): other = lax.ppermute(payload, 'sp', swap(sp, bits[0]))  3.45 us
    pallas_call x1, Pallas kernels, whole(): call(functools.partial(early_kernel, log_length=log_length, blocks=count)...  2.68 us
  transfers between devices with their start and end apart: 11, of which 7 were waited for; matrix products, arithmetic and copies ran while one was open for 0% of the time, Pallas kernels for 12%

profile of v3, /device:TPU:0, one launch (start us, length us, event | category | flops | bytes accessed | tf_op | source)
XLA Modules:
  0.0 60.9 jit_solution(7692863024116854500)
XLA Ops:
  0.6 1.3 %shard_map.78 = (bf16[64,4096]{1,0:T(8,128)(2,1)S(1)}, bf16[40,4096]{1,0:T(8,128)(2,1)S(1)}) custom-call(bf16[128,4096]{1,0:T(8,128)(2,1)} %tokens.3), custom_call_target="tpu_custom_call" | custom-call | tf_op jit(solution)/shard_map/pallas_call | solution.py:300
  2.0 3.1 %collective-permute-start.5 = (bf16[64,4096]{1,0:T(8,128)(2,1)S(1)}, bf16[64,4096]{1,0:T(8,128)(2,1)S(1)}, u32[]{:S(2)}, u32[]{:S(2)}) collective-permute-start(bf16[64,4096]{1,0:T(8,128)(2,1)S(1)} %get-tuple-element.18), channel_id=1, source_target_pairs={{0,2},{1,3},{2,0},{3,1},{4,6},{5,7},{6,4},{7,5},{8,10},{9,11},{10,... | collective-permute-start | bytes 1572872 | tf_op jit(solution)/shard_map/ppermute | solution.py:309
  5.0 0.0 collective-permute-start.2
  5.0 11.9 %collective-permute-done.5.refs_2_ = bf16[64,4096]{1,0:T(8,128)(2,1)S(1)} collective-permute-done((bf16[64,4096]{1,0:T(8,128)(2,1)S(1)}, bf16[64,4096]{1,0:T(8,128)(2,1)S(1)}, u32[]{:S(2)}, u32[]{:S(2)}) %collective-permute-start.5) | collective-permute-done | bytes 524320 | tf_op jit(solution)/shard_map/ppermute | solution.py:309
  16.9 0.0 collective-permute-start.6
  16.9 0.9 %shard_map.80 = bf16[24,4096]{1,0:T(8,128)(2,1)S(1)} custom-call(bf16[128,4096]{1,0:T(8,128)(2,1)} %tokens.3), custom_call_target="tpu_custom_call" | custom-call | tf_op jit(solution)/shard_map/pallas_call | solution.py:300
  17.9 1.8 %collective-permute-start.3 = (bf16[24,4096]{1,0:T(8,128)(2,1)S(1)}, bf16[24,4096]{1,0:T(8,128)(2,1)S(1)}, u32[]{:S(2)}, u32[]{:S(2)}) collective-permute-start(bf16[24,4096]{1,0:T(8,128)(2,1)S(1)} %shard_map.80), channel_id=1, source_target_pairs={{0,2},{1,3},{2,0},{3,1},{4,6},{5,7},{6,4},{7,5},{8,10},{9,11},{10,... | collective-permute-start | bytes 589832 | tf_op jit(solution)/shard_map/ppermute | solution.py:309
  19.7 0.3 collective-permute-start
  20.0 5.7 %collective-permute-done.3.refs_0_ = bf16[24,4096]{1,0:T(8,128)(2,1)S(1)} collective-permute-done((bf16[24,4096]{1,0:T(8,128)(2,1)S(1)}, bf16[24,4096]{1,0:T(8,128)(2,1)S(1)}, u32[]{:S(2)}, u32[]{:S(2)}) %collective-permute-start.3) | collective-permute-done | bytes 196640 | tf_op jit(solution)/shard_map/ppermute | solution.py:309
  25.7 0.0 collective-permute-start.4
  25.7 6.6 %collective-permute-done.xa = bf16[40,4096]{1,0:T(8,128)(2,1)S(1)} collective-permute-done((bf16[40,4096]{1,0:T(8,128)(2,1)S(1)}, bf16[40,4096]{1,0:T(8,128)(2,1)S(1)}, u32[]{:S(2)}, u32[]{:S(2)}) %collective-permute-start) | collective-permute-done | bytes 327712 | tf_op jit(solution)/shard_map/ppermute | solution.py:309
  32.3 0.0 copy-start
  32.3 2.2 %copy-done = bf16[4096,512]{1,0:T(8,128)(2,1)S(1)} copy-done((bf16[4096,512]{1,0:T(8,128)(2,1)S(1)}, bf16[4096,512]{1,0:T(8,128)(2,1)}, u32[]{:S(2)}) %copy-start) | copy-done | bytes 4194328
  34.5 1.6 %copy-done.3 = bf16[4096,256]{1,0:T(8,128)(2,1)S(1)} copy-done((bf16[4096,256]{1,0:T(8,128)(2,1)S(1)}, bf16[4096,256]{1,0:T(8,128)(2,1)}, u32[]{:S(2)}) %copy-start.3) | copy-done | bytes 2097176
  36.1 2.7 %shard_map.81 = (f32[128,256]{1,0:T(8,128)S(1)}, f32[128,256]{1,0:T(8,128)S(1)}, f32[128,256]{1,0:T(8,128)S(1)}, f32[128,256]{1,0:T(8,128)S(1)}, f32[1,256]{1,0:...) custom-call(bf16[24,4096]{1,0:T(8,128)(2,1)S(1)} %collective-permute-done.3.refs_0_, ...), custom_call_target="tpu_custom_call" | custom-call | flops 1476395008 | tf_op jit(solution)/shard_map/pallas_call | solution.py:330
  38.8 0.0 collective-permute-done.2.x1
  38.8 0.2 copy-done.4
  39.0 0.2 copy-done.5
  39.2 3.5 %shard_map.79 = (f32[128,256]{1,0:T(8,128)S(1)}, f32[1,256]{1,0:T(1,128)S(1)}) custom-call(bf16[128,4096]{1,0:T(8,128)(2,1)S(1)} %copy-done.5, bf16[128,4096]{1,0:T(8,128)(2,1)S(1)} %collective-permute-done.2.x1, bf16[4096,256]{1,0:T(8,128)(2,1)S(1)} %copy-done.2, bf16[4096,512]{1,0:T(8,128)(2,1)S(1)} %copy-done.1, bf16[4096,256]{1,0:T(8,128)(2,1)S(1)} %copy-done.4, ...), custom_call_target="tpu_custom_call" | custom-call | flops 2147483648 | tf_op jit(solution)/shard_map/pallas_call | solution.py:312
  42.7 0.0 copy-start.7
  42.7 2.1 %shard_map.82.refs_0_ = bf16[144,256]{1,0:T(8,128)(2,1)S(1)} custom-call(bf16[40,4096]{1,0:T(8,128)(2,1)S(1)} %collective-permute-done.xa, bf16[40,4096]{1,0:T(8,128)(2,1)S(1)} %collective-permute-done.1.xb, bf16[4096,256]{1,0:T(8,128)(2,1)S(1)} %copy-done.2, bf16[4096,512]{1,0:T(8,128)(2,1)S(1)} %copy-done.1, bf16[4096,256]{1,0:T(8,128)(2,1)S(1)} %copy-done.4, ...), custom_call_target="tpu_custom_call" | custom-call | flops 671088640 | tf_op jit(solution)/shard_map/pallas_call | solution.py:339
  44.8 1.8 %collective-permute-start.7 = (bf16[144,256]{1,0:T(8,128)(2,1)S(1)}, bf16[144,256]{1,0:T(8,128)(2,1)S(1)}, u32[]{:S(2)}, u32[]{:S(2)}) collective-permute-start(bf16[144,256]{1,0:T(8,128)(2,1)S(1)} %shard_map.82.refs_0_), channel_id=1, source_target_pairs={{0,4},{4,0},{8,12},{12,8},{16,20},{20,16},{24,28},{28,24},{1,5},{5... | collective-permute-start | bytes 221192 | tf_op jit(solution)/shard_map/ppermute | solution.py:359
  46.6 1.6 %collective-permute-start.8 = (bf16[144,256]{1,0:T(8,128)(2,1)S(1)}, bf16[144,256]{1,0:T(8,128)(2,1)S(1)}, u32[]{:S(2)}, u32[]{:S(2)}) collective-permute-start(bf16[144,256]{1,0:T(8,128)(2,1)S(1)} %shard_map.82.refs_0_), channel_id=1, source_target_pairs={{0,8},{4,12},{8,0},{12,4},{16,24},{20,28},{24,16},{28,20},{1,9},{5... | collective-permute-start | bytes 221192 | tf_op jit(solution)/shard_map/ppermute | solution.py:359
  48.2 0.2 collective-permute-start.9
  48.4 0.1 shard_map.77.asked
  48.4 1.1 %collective-permute-done.7.refs_1_ = bf16[144,256]{1,0:T(8,128)(2,1)S(1)} collective-permute-done((bf16[144,256]{1,0:T(8,128)(2,1)S(1)}, bf16[144,256]{1,0:T(8,128)(2,1)S(1)}, u32[]{:S(2)}, u32[]{:S(2)}) %collective-permute-start.7) | collective-permute-done | bytes 73760 | tf_op jit(solution)/shard_map/ppermute | solution.py:359
  49.6 1.7 %collective-permute-done.8.refs_2_ = bf16[144,256]{1,0:T(8,128)(2,1)S(1)} collective-permute-done((bf16[144,256]{1,0:T(8,128)(2,1)S(1)}, bf16[144,256]{1,0:T(8,128)(2,1)S(1)}, u32[]{:S(2)}, u32[]{:S(2)}) %collective-permute-start.8) | collective-permute-done | bytes 73760 | tf_op jit(solution)/shard_map/ppermute | solution.py:359
  51.3 2.1 %collective-permute-done.9.refs_3_ = bf16[144,256]{1,0:T(8,128)(2,1)S(1)} collective-permute-done((bf16[144,256]{1,0:T(8,128)(2,1)S(1)}, bf16[144,256]{1,0:T(8,128)(2,1)S(1)}, u32[]{:S(2)}, u32[]{:S(2)}) %collective-permute-start.9) | collective-permute-done | bytes 73760 | tf_op jit(solution)/shard_map/ppermute | solution.py:359
  53.4 0.3 shard_map.83
  53.7 2.7 %collective-permute-start.10 = (bf16[144,256]{1,0:T(8,128)(2,1)S(1)}, bf16[144,256]{1,0:T(8,128)(2,1)S(1)}, u32[]{:S(2)}, u32[]{:S(2)}) collective-permute-start(bf16[144,256]{1,0:T(8,128)(2,1)S(1)} %get-tuple-element.28.mine), channel_id=1, source_target_pairs={{0,16},{4,20},{8,24},{12,28},{16,0},{20,4},{24,8},{28,12},{1,17},{... | collective-permute-start | bytes 221192 | tf_op jit(solution)/shard_map/ppermute | solution.py:365
  56.4 3.5 %collective-permute-done.10.other = bf16[144,256]{1,0:T(8,128)(2,1)S(1)} collective-permute-done((bf16[144,256]{1,0:T(8,128)(2,1)S(1)}, bf16[144,256]{1,0:T(8,128)(2,1)S(1)}, u32[]{:S(2)}, u32[]{:S(2)}) %collective-permute-start.10) | collective-permute-done | bytes 73760 | tf_op jit(solution)/shard_map/ppermute | solution.py:365
  59.8 1.0 %shard_map.84 = (bf16[4,8,128]{2,1,0:T(8,128)(2,1)}, bf16[4,128]{1,0:T(4,128)(2,1)}) custom-call(f32[8,256]{1,0:T(8,128)S(1)} %shard_map.77.asked, bf16[144,256]{1,0:T(8,128)(2,1)S(1)} %get-tuple-element.28.mine, bf16[144,256]{1,0:T(8,128)(2,1)S(1)} %collective-permute-done.10.other, f32[128,256]{1,0:T(8,128)S(1)} %get-tuple-element.29.exact), custom_call_target="tpu_custom_call" | custom-call | tf_op jit(solution)/shard_map/pallas_call | solution.py:366
  (14 shorter events, 0.0 us)
Async XLA Ops:
  0.6 31.7 %copy-start.6 = (f32[256]{0:T(256)S(1)}, f32[256]{0:T(256)}, u32[]{:S(2)}) copy-start(f32[256]{0:T(256)} %param.10) | copy-start | bytes 3076
  0.6 31.7 %copy-start.2 = (bf16[4096,256]{1,0:T(8,128)(2,1)S(1)}, bf16[4096,256]{1,0:T(8,128)(2,1)}, u32[]{:S(2)}) copy-start(bf16[4096,256]{1,0:T(8,128)(2,1)} %wk.3) | copy-start | bytes 6291460
  2.0 15.0 %collective-permute-start.5 = (bf16[64,4096]{1,0:T(8,128)(2,1)S(1)}, bf16[64,4096]{1,0:T(8,128)(2,1)S(1)}, u32[]{:S(2)}, u32[]{:S(2)}) collective-permute-start(bf16[64,4096]{1,0:T(8,128)(2,1)S(1)} %get-tuple-element.18), channel_id=1, source_target_pairs={{0,2},{1,3},{2,0},{3,1},{4,6},{5,7},{6,4},{7,5},{8,10},{9,11},{10,... | collective-permute-start | bytes 1572872 | tf_op jit(solution)/shard_map/ppermute | solution.py:309
  5.0 33.8 %collective-permute-start.2 = (bf16[128,4096]{1,0:T(8,128)(2,1)}, bf16[128,4096]{1,0:T(8,128)(2,1)S(1)}, u32[]{:S(2)}, u32[]{:S(2)}) collective-permute-start(bf16[128,4096]{1,0:T(8,128)(2,1)} %tokens.3), channel_id=1, source_target_pairs={{0,1},{1,0},{2,3},{3,2},{4,5},{5,4},{6,7},{7,6},{8,9},{9,8},{10,11... | collective-permute-start | bytes 3145736 | tf_op jit(solution)/shard_map/ppermute | solution.py:310
  16.9 15.4 %collective-permute-start.6 = (bf16[64,4096]{1,0:T(8,128)(2,1)S(1)}, bf16[64,4096]{1,0:T(8,128)(2,1)S(1)}, u32[]{:S(2)}, u32[]{:S(2)}) collective-permute-start(bf16[64,4096]{1,0:T(8,128)(2,1)S(1)} %collective-permute-done.5.refs_2_), channel_id=1, source_target_pairs={{0,1},{1,0},{2,3},{3,2},{4,5},{5,4},{6,7},{7,6},{8,9},{9,8},{10,11... | collective-permute-start | bytes 1572872 | tf_op jit(solution)/shard_map/ppermute | solution.py:324
  17.9 7.8 %collective-permute-start.3 = (bf16[24,4096]{1,0:T(8,128)(2,1)S(1)}, bf16[24,4096]{1,0:T(8,128)(2,1)S(1)}, u32[]{:S(2)}, u32[]{:S(2)}) collective-permute-start(bf16[24,4096]{1,0:T(8,128)(2,1)S(1)} %shard_map.80), channel_id=1, source_target_pairs={{0,2},{1,3},{2,0},{3,1},{4,6},{5,7},{6,4},{7,5},{8,10},{9,11},{10,... | collective-permute-start | bytes 589832 | tf_op jit(solution)/shard_map/ppermute | solution.py:309
  19.7 12.6 %collective-permute-start = (bf16[40,4096]{1,0:T(8,128)(2,1)S(1)}, bf16[40,4096]{1,0:T(8,128)(2,1)S(1)}, u32[]{:S(2)}, u32[]{:S(2)}) collective-permute-start(bf16[40,4096]{1,0:T(8,128)(2,1)S(1)} %get-tuple-element.16), channel_id=1, source_target_pairs={{0,2},{1,3},{2,0},{3,1},{4,6},{5,7},{6,4},{7,5},{8,10},{9,11},{10,... | collective-permute-start | bytes 983048 | tf_op jit(solution)/shard_map/ppermute | solution.py:309
  25.7 6.6 %collective-permute-start.4 = (bf16[24,4096]{1,0:T(8,128)(2,1)S(1)}, bf16[24,4096]{1,0:T(8,128)(2,1)S(1)}, u32[]{:S(2)}, u32[]{:S(2)}) collective-permute-start(bf16[24,4096]{1,0:T(8,128)(2,1)S(1)} %collective-permute-done.3.refs_0_), channel_id=1, source_target_pairs={{0,1},{1,0},{2,3},{3,2},{4,5},{5,4},{6,7},{7,6},{8,9},{9,8},{10,11... | collective-permute-start | bytes 589832 | tf_op jit(solution)/shard_map/ppermute | solution.py:324
  32.3 10.4 %collective-permute-start.1 = (bf16[40,4096]{1,0:T(8,128)(2,1)S(1)}, bf16[40,4096]{1,0:T(8,128)(2,1)S(1)}, u32[]{:S(2)}, u32[]{:S(2)}) collective-permute-start(bf16[40,4096]{1,0:T(8,128)(2,1)S(1)} %collective-permute-done.xa), channel_id=1, source_target_pairs={{0,1},{1,0},{2,3},{3,2},{4,5},{5,4},{6,7},{7,6},{8,9},{9,8},{10,11... | collective-permute-start | bytes 983048 | tf_op jit(solution)/shard_map/ppermute | solution.py:324
  32.3 2.2 %copy-start = (bf16[4096,512]{1,0:T(8,128)(2,1)S(1)}, bf16[4096,512]{1,0:T(8,128)(2,1)}, u32[]{:S(2)}) copy-start(bf16[4096,512]{1,0:T(8,128)(2,1)} %wv.3) | copy-start | bytes 12582916
  34.5 1.6 %copy-start.3 = (bf16[4096,256]{1,0:T(8,128)(2,1)S(1)}, bf16[4096,256]{1,0:T(8,128)(2,1)}, u32[]{:S(2)}) copy-start(bf16[4096,256]{1,0:T(8,128)(2,1)} %wd.3) | copy-start | bytes 6291460
  36.1 2.7 %copy-start.1 = (bf16[4096,512]{1,0:T(8,128)(2,1)S(1)}, bf16[4096,512]{1,0:T(8,128)(2,1)}, u32[]{:S(2)}) copy-start(bf16[4096,512]{1,0:T(8,128)(2,1)} %wv.3) | copy-start | bytes 12582916
  36.1 2.9 %copy-start.4 = (bf16[4096,256]{1,0:T(8,128)(2,1)S(1)}, bf16[4096,256]{1,0:T(8,128)(2,1)}, u32[]{:S(2)}) copy-start(bf16[4096,256]{1,0:T(8,128)(2,1)} %wd.3) | copy-start | bytes 6291460
  36.1 3.1 %copy-start.5 = (bf16[128,4096]{1,0:T(8,128)(2,1)S(1)}, bf16[128,4096]{1,0:T(8,128)(2,1)}, u32[]{:S(2)}) copy-start(bf16[128,4096]{1,0:T(8,128)(2,1)} %tokens.3) | copy-start | bytes 3145732
  42.7 5.7 %copy-start.7 = (bf16[4,64]{1,0:T(4,128)(2,1)S(1)}, bf16[4,64]{1,0:T(4,128)(2,1)}, u32[]{:S(2)}) copy-start(bf16[4,64]{1,0:T(4,128)(2,1)} %question.1) | copy-start | bytes 1540
  44.8 4.7 %collective-permute-start.7 = (bf16[144,256]{1,0:T(8,128)(2,1)S(1)}, bf16[144,256]{1,0:T(8,128)(2,1)S(1)}, u32[]{:S(2)}, u32[]{:S(2)}) collective-permute-start(bf16[144,256]{1,0:T(8,128)(2,1)S(1)} %shard_map.82.refs_0_), channel_id=1, source_target_pairs={{0,4},{4,0},{8,12},{12,8},{16,20},{20,16},{24,28},{28,24},{1,5},{5... | collective-permute-start | bytes 221192 | tf_op jit(solution)/shard_map/ppermute | solution.py:359
  46.6 4.7 %collective-permute-start.8 = (bf16[144,256]{1,0:T(8,128)(2,1)S(1)}, bf16[144,256]{1,0:T(8,128)(2,1)S(1)}, u32[]{:S(2)}, u32[]{:S(2)}) collective-permute-start(bf16[144,256]{1,0:T(8,128)(2,1)S(1)} %shard_map.82.refs_0_), channel_id=1, source_target_pairs={{0,8},{4,12},{8,0},{12,4},{16,24},{20,28},{24,16},{28,20},{1,9},{5... | collective-permute-start | bytes 221192 | tf_op jit(solution)/shard_map/ppermute | solution.py:359
  48.2 5.3 %collective-permute-start.9 = (bf16[144,256]{1,0:T(8,128)(2,1)S(1)}, bf16[144,256]{1,0:T(8,128)(2,1)S(1)}, u32[]{:S(2)}, u32[]{:S(2)}) collective-permute-start(bf16[144,256]{1,0:T(8,128)(2,1)S(1)} %shard_map.82.refs_0_), channel_id=1, source_target_pairs={{0,12},{4,8},{8,4},{12,0},{16,28},{20,24},{24,20},{28,16},{1,13},{... | collective-permute-start | bytes 221192 | tf_op jit(solution)/shard_map/ppermute | solution.py:359
  53.7 6.1 %collective-permute-start.10 = (bf16[144,256]{1,0:T(8,128)(2,1)S(1)}, bf16[144,256]{1,0:T(8,128)(2,1)S(1)}, u32[]{:S(2)}, u32[]{:S(2)}) collective-permute-start(bf16[144,256]{1,0:T(8,128)(2,1)S(1)} %get-tuple-element.28.mine), channel_id=1, source_target_pairs={{0,16},{4,20},{8,24},{12,28},{16,0},{20,4},{24,8},{28,12},{1,17},{... | collective-permute-start | bytes 221192 | tf_op jit(solution)/shard_map/ppermute | solution.py:365

commit v4 on v3

--- a/solution.py
+++ b/solution.py
@@ -12,7 +12,8 @@
 CUE_WIDTH = 64
 DV = 128
 DECAY_TAU = 16.0
-ROW_PARTS = (3, 8, 5)
+ROW_PARTS = (3, 8, 3, 2)
+LATE = 2
 VMEM_LIMIT = 8 * 1024 * 1024
 
 
@@ -71,10 +72,10 @@
     return parts[0] if len(parts) == 1 else jnp.concatenate(parts, axis=1)
 
 
-def payload_sds(heads):
-    pad = -(3 + 3 * heads) % 16
+def payload_sds(heads, heard):
+    rows = 3 + 3 * heads if heard else 3
     width = max(heads * CUE_WIDTH, DV)
-    return jax.ShapeDtypeStruct((DV + 3 + 3 * heads + pad, width), BF16)
+    return jax.ShapeDtypeStruct((DV + rows + -rows % 8, width), BF16)
 
 
 def split(exact):
@@ -177,14 +178,17 @@
         lo = hi
 
 
-def late_kernel(xa, xb, wk, wv, wd, off, *refs, log_length, blocks, here, parts):
+def late_kernel(*refs, log_length, blocks, late, here, parts):
+    x = jnp.concatenate([ref[...] for ref in refs[: 2 * late]], axis=0)
+    wk, wv, wd, off = refs[2 * late : 2 * late + 4]
+    refs = refs[2 * late + 4 :]
     states = refs[: len(blocks)]
     totals = refs[len(blocks) : 2 * len(blocks)]
     out = refs[2 * len(blocks)]
     place = lax.axis_index("tp")
     core = lax.rem(place, 2)
     chip = lax.div(place, 2)
-    rows = xa.shape[0]
+    rows = x.shape[0] // 2
 
     def position(block):
         if block is None:
@@ -193,7 +197,6 @@
         parity = core if same else 1 - core
         return lax.bitwise_xor(chip, bit) * (2 * parts) + parity * parts + part
 
-    x = jnp.concatenate([xa[...], xb[...]], axis=0)
     keys, values, log_decay = project(x, wk, wv, wd, off[...], log_length)
     after = later_within(log_decay, [rows, rows])
     own = [
@@ -238,7 +241,8 @@
         total = total + t
     exact[...] = state
     heads = key_cols // CUE_WIDTH
-    pack(out, state, total, against(asked[...], state)[:heads])
+    last = out.shape[0] > DV + 8
+    pack(out, state, total, against(asked[...], state)[:heads] if last else None)
 
 
 def final_kernel(asked, mine, other, exact, cache, read, *, bit):
@@ -322,9 +326,10 @@
     pairs = {}
     for bit, part in far:
         pairs[bit, part] = (far[bit, part], lax.ppermute(far[bit, part], "tp", swap(tp, 1)))
-    last = (tp // 2 - 1, len(cuts) - 1)
+    early = len(cuts) - LATE
+    last = [(tp // 2 - 1, early + n) for n in range(LATE)]
     for bit in range(1, tp // 2):
-        taken = [key for key in pairs if key[0] == bit and key != last]
+        taken = [key for key in pairs if key[0] == bit and key not in last]
         inputs = [x for key in taken for x in pairs[key]]
         count = len(inputs)
         outs = call(
@@ -341,13 +346,14 @@
             late_kernel,
             log_length=log_length,
             blocks=tuple(blocks),
-            here=last,
+            late=LATE,
+            here=last[0],
             parts=len(cuts),
         ),
-        payload_sds(heads),
-        [VM] * (6 + 2 * len(blocks)),
-        flops=4 * pairs[last][0].shape[0] * width * cols,
-    )(*pairs[last], wk, wv, wd, offset, *states, *totals)
+        payload_sds(heads, sp == 2),
+        [VM] * (2 * LATE + 4 + 2 * len(blocks)),
+        flops=4 * (edges[-1] - edges[early]) * width * cols,
+    )(*(pairs[key][side] for side in (0, 1) for key in last), wk, wv, wd, offset, *states, *totals)
 
     bits = [1 << n for n in range(sp.bit_length() - 1)]
     while len(bits) > 1:
@@ -359,7 +365,7 @@
             others.append(lax.ppermute(payload, "sp", swap(sp, far_bits)))
         payload, exact = call(
             functools.partial(merge_kernel, bits=tuple(group)),
-            (payload_sds(heads), state_sds),
+            (payload_sds(heads, len(bits) == 1), state_sds),
             [VM] * (2 + len(others)),
         )(asked, payload, *others)
     other = lax.ppermute(payload, "sp", swap(sp, bits[0]))
@@ -381,10 +387,14 @@
         P("tp", None),
     )
     out_specs = (P("tp", "sp", None), P("tp", None))
-    return jax.shard_map(
+    step = jax.shard_map(
         functools.partial(whole, sp, tp),
         mesh=mesh,
         in_specs=in_specs,
         out_specs=out_specs,
         check_vma=False,
     )
+    bit = 1
+    while 4 * bit < sp:
+        bit *= 4
+    return step

time: 61.1 us -> 63.6 us (1.041)
  starting transfers between devices: 11.4 us -> 13.8 us
  local copies, waits for them, and re-layouts: 4.17 us -> 5.02 us
  waiting for transfers between devices: 32.7 us -> 32 us
    ppermute x3 -> x4, starting transfers between devices: 5.15 us -> 6.48 us  [whole(): far[bit, part] = lax.ppermute(piece, 'tp', swap(tp, 2 * bit))]
    ppermute x3 -> x4, waiting for transfers between devices: 24.2 us -> 23 us  [whole(): far[bit, part] = lax.ppermute(piece, 'tp', swap(tp, 2 * bit))]
    unnamed x16, local copies, waits for them, and re-layouts: 4.17 us -> 5.02 us
  transfers between devices with their start and end apart: 11 -> 13, of which waited for: 7 -> 6; matrix products, arithmetic and copies ran while one was open for 0% -> 0% of each run, Pallas kernels for 12% -> 13%
where the time goes in v4:
time: 63.6 us; the launch traced here: 63.4 us
  waiting for transfers between devices  32 us (50%)
  starting transfers between devices  13.8 us (22%)
  Pallas kernels  11.8 us (19%)
  local copies, waits for them, and re-layouts  5.02 us (8%)
  between operations  0.77 us (1%)
    ppermute x4, waiting for transfers between devices, whole(): far[bit, part] = lax.ppermute(piece, 'tp', swap(tp, 2 * bit))  23 us
    ppermute x4, starting transfers between devices, whole(): far[bit, part] = lax.ppermute(piece, 'tp', swap(tp, 2 * bit))  6.48 us
    unnamed x16, local copies, waits for them, and re-layouts  5.02 us
    ppermute x3, waiting for transfers between devices, whole(): others.append(lax.ppermute(payload, 'sp', swap(sp, far_bits)))  4.97 us
    ppermute x1, waiting for transfers between devices, whole(): other = lax.ppermute(payload, 'sp', swap(sp, bits[0]))  3.96 us
    ppermute x3, starting transfers between devices, whole(): others.append(lax.ppermute(payload, 'sp', swap(sp, far_bits)))  3.55 us
    pallas_call x1, Pallas kernels, whole(): call(functools.partial(near_kernel, log_length=log_length), (state_sds, t...  3.4 us
    pallas_call x1, Pallas kernels, whole(): call(functools.partial(early_kernel, log_length=log_length, blocks=count)...  2.67 us
  transfers between devices with their start and end apart: 13, of which 6 were waited for; matrix products, arithmetic and copies ran while one was open for 0% of the time, Pallas kernels for 13%

profile of v4, /device:TPU:0, one launch (start us, length us, event | category | flops | bytes accessed | tf_op | source)
XLA Modules:
  0.0 63.4 jit_solution(16484490819322428612)
XLA Ops:
  0.6 0.6 collective-permute-start.4
  1.2 1.2 %shard_map.78 = (bf16[64,4096]{1,0:T(8,128)(2,1)S(1)}, bf16[24,4096]{1,0:T(8,128)(2,1)S(1)}, bf16[16,4096]{1,0:T(8,128)(2,1)S(1)}) custom-call(bf16[128,4096]{1,0:T(8,128)(2,1)} %tokens.3), custom_call_target="tpu_custom_call" | custom-call | tf_op jit(solution)/shard_map/pallas_call | solution.py:304
  2.4 2.6 %collective-permute-start.7 = (bf16[64,4096]{1,0:T(8,128)(2,1)S(1)}, bf16[64,4096]{1,0:T(8,128)(2,1)S(1)}, u32[]{:S(2)}, u32[]{:S(2)}) collective-permute-start(bf16[64,4096]{1,0:T(8,128)(2,1)S(1)} %get-tuple-element.20), channel_id=1, source_target_pairs={{0,2},{1,3},{2,0},{3,1},{4,6},{5,7},{6,4},{7,5},{8,10},{9,11},{10,... | collective-permute-start | bytes 1572872 | tf_op jit(solution)/shard_map/ppermute | solution.py:313
  5.1 12.4 %collective-permute-done.7.refs_2_ = bf16[64,4096]{1,0:T(8,128)(2,1)S(1)} collective-permute-done((bf16[64,4096]{1,0:T(8,128)(2,1)S(1)}, bf16[64,4096]{1,0:T(8,128)(2,1)S(1)}, u32[]{:S(2)}, u32[]{:S(2)}) %collective-permute-start.7) | collective-permute-done | bytes 524320 | tf_op jit(solution)/shard_map/ppermute | solution.py:313
  17.5 0.9 %shard_map.80 = bf16[24,4096]{1,0:T(8,128)(2,1)S(1)} custom-call(bf16[128,4096]{1,0:T(8,128)(2,1)} %tokens.3), custom_call_target="tpu_custom_call" | custom-call | tf_op jit(solution)/shard_map/pallas_call | solution.py:304
  18.5 1.8 %collective-permute-start.5 = (bf16[24,4096]{1,0:T(8,128)(2,1)S(1)}, bf16[24,4096]{1,0:T(8,128)(2,1)S(1)}, u32[]{:S(2)}, u32[]{:S(2)}) collective-permute-start(bf16[24,4096]{1,0:T(8,128)(2,1)S(1)} %shard_map.80), channel_id=1, source_target_pairs={{0,2},{1,3},{2,0},{3,1},{4,6},{5,7},{6,4},{7,5},{8,10},{9,11},{10,... | collective-permute-start | bytes 589832 | tf_op jit(solution)/shard_map/ppermute | solution.py:313
  20.3 0.3 collective-permute-start
  20.6 1.7 %collective-permute-start.1 = (bf16[16,4096]{1,0:T(8,128)(2,1)S(1)}, bf16[16,4096]{1,0:T(8,128)(2,1)S(1)}, u32[]{:S(2)}, u32[]{:S(2)}) collective-permute-start(bf16[16,4096]{1,0:T(8,128)(2,1)S(1)} %get-tuple-element.18), channel_id=1, source_target_pairs={{0,2},{1,3},{2,0},{3,1},{4,6},{5,7},{6,4},{7,5},{8,10},{9,11},{10,... | collective-permute-start | bytes 393224 | tf_op jit(solution)/shard_map/ppermute | solution.py:313
  22.3 10.6 %collective-permute-done.1.refs_1_ = bf16[16,4096]{1,0:T(8,128)(2,1)S(1)} collective-permute-done((bf16[16,4096]{1,0:T(8,128)(2,1)S(1)}, bf16[16,4096]{1,0:T(8,128)(2,1)S(1)}, u32[]{:S(2)}, u32[]{:S(2)}) %collective-permute-start.1) | collective-permute-done | bytes 131104 | tf_op jit(solution)/shard_map/ppermute | solution.py:313
  32.9 0.0 collective-permute-start.3
  32.9 0.5 collective-permute-start.6
  33.4 0.1 collective-permute-start.2
  33.5 0.0 collective-permute-done.4.x1
  33.5 0.0 copy-start
  33.5 2.2 %copy-done = bf16[4096,512]{1,0:T(8,128)(2,1)S(1)} copy-done((bf16[4096,512]{1,0:T(8,128)(2,1)S(1)}, bf16[4096,512]{1,0:T(8,128)(2,1)}, u32[]{:S(2)}) %copy-start) | copy-done | bytes 4194328
  35.7 1.6 %copy-done.3 = bf16[4096,256]{1,0:T(8,128)(2,1)S(1)} copy-done((bf16[4096,256]{1,0:T(8,128)(2,1)S(1)}, bf16[4096,256]{1,0:T(8,128)(2,1)}, u32[]{:S(2)}) %copy-start.3) | copy-done | bytes 2097176
  37.3 1.2 %copy-done.5 = bf16[128,4096]{1,0:T(8,128)(2,1)S(1)} copy-done((bf16[128,4096]{1,0:T(8,128)(2,1)S(1)}, bf16[128,4096]{1,0:T(8,128)(2,1)}, u32[]{:S(2)}) %copy-start.5) | copy-done | bytes 1048600
  38.5 3.4 %shard_map.79 = (f32[128,256]{1,0:T(8,128)S(1)}, f32[1,256]{1,0:T(1,128)S(1)}) custom-call(bf16[128,4096]{1,0:T(8,128)(2,1)S(1)} %copy-done.5, bf16[128,4096]{1,0:T(8,128)(2,1)S(1)} %collective-permute-done.4.x1, bf16[4096,256]{1,0:T(8,128)(2,1)S(1)} %copy-done.2, bf16[4096,512]{1,0:T(8,128)(2,1)S(1)} %copy-done, bf16[4096,256]{1,0:T(8,128)(2,1)S(1)} %copy-done.3, ...), custom_call_target="tpu_custom_call" | custom-call | flops 2147483648 | tf_op jit(solution)/shard_map/pallas_call | solution.py:316
  41.9 2.7 %shard_map.81 = (f32[128,256]{1,0:T(8,128)S(1)}, f32[128,256]{1,0:T(8,128)S(1)}, f32[128,256]{1,0:T(8,128)S(1)}, f32[128,256]{1,0:T(8,128)S(1)}, f32[1,256]{1,0:...) custom-call(bf16[24,4096]{1,0:T(8,128)(2,1)S(1)} %collective-permute-done.5.refs_0_, ...), custom_call_target="tpu_custom_call" | custom-call | flops 1476395008 | tf_op jit(solution)/shard_map/pallas_call | solution.py:335
  44.6 0.0 copy-start.7
  44.7 2.2 %shard_map.82.refs_0_ = bf16[136,256]{1,0:T(8,128)(2,1)S(1)} custom-call(bf16[24,4096]{1,0:T(8,128)(2,1)S(1)} %collective-permute-done.refs_0_, bf16[16,4096]{1,0:T(8,128)(2,1)S(1)} %collective-permute-done.1.refs_1_, bf16[24,4096]{1,0:T(8,128)(2,1)S(1)} %collective-permute-done.2.refs_2_, bf16[16,4096]{1,0:T(8,128)(2,1)S(1)} %collective-permute-done.3.refs_3_, ...), custom_call_target="tpu_custom_call" | custom-call | flops 671088640 | tf_op jit(solution)/shard_map/pallas_call | solution.py:344
  46.8 1.9 %collective-permute-start.10 = (bf16[136,256]{1,0:T(8,128)(2,1)S(1)}, bf16[136,256]{1,0:T(8,128)(2,1)S(1)}, u32[]{:S(2)}, u32[]{:S(2)}) collective-permute-start(bf16[136,256]{1,0:T(8,128)(2,1)S(1)} %shard_map.82.refs_0_), channel_id=1, source_target_pairs={{0,8},{4,12},{8,0},{12,4},{16,24},{20,28},{24,16},{28,20},{1,9},{5... | collective-permute-start | bytes 208904 | tf_op jit(solution)/shard_map/ppermute | solution.py:365
  48.7 1.4 %collective-permute-start.11 = (bf16[136,256]{1,0:T(8,128)(2,1)S(1)}, bf16[136,256]{1,0:T(8,128)(2,1)S(1)}, u32[]{:S(2)}, u32[]{:S(2)}) collective-permute-start(bf16[136,256]{1,0:T(8,128)(2,1)S(1)} %shard_map.82.refs_0_), channel_id=1, source_target_pairs={{0,12},{4,8},{8,4},{12,0},{16,28},{20,24},{24,20},{28,16},{1,13},{... | collective-permute-start | bytes 208904 | tf_op jit(solution)/shard_map/ppermute | solution.py:365
  50.1 0.3 collective-permute-start.9
  50.4 0.1 shard_map.77.asked
  50.5 1.0 %collective-permute-done.10.refs_2_ = bf16[136,256]{1,0:T(8,128)(2,1)S(1)} collective-permute-done((bf16[136,256]{1,0:T(8,128)(2,1)S(1)}, bf16[136,256]{1,0:T(8,128)(2,1)S(1)}, u32[]{:S(2)}, u32[]{:S(2)}) %collective-permute-start.10) | collective-permute-done | bytes 69664 | tf_op jit(solution)/shard_map/ppermute | solution.py:365
  51.5 2.7 %collective-permute-done.11.refs_3_ = bf16[136,256]{1,0:T(8,128)(2,1)S(1)} collective-permute-done((bf16[136,256]{1,0:T(8,128)(2,1)S(1)}, bf16[136,256]{1,0:T(8,128)(2,1)S(1)}, u32[]{:S(2)}, u32[]{:S(2)}) %collective-permute-start.11) | collective-permute-done | bytes 69664 | tf_op jit(solution)/shard_map/ppermute | solution.py:365
  54.2 1.3 %collective-permute-done.9.refs_1_ = bf16[136,256]{1,0:T(8,128)(2,1)S(1)} collective-permute-done((bf16[136,256]{1,0:T(8,128)(2,1)S(1)}, bf16[136,256]{1,0:T(8,128)(2,1)S(1)}, u32[]{:S(2)}, u32[]{:S(2)}) %collective-permute-start.9) | collective-permute-done | bytes 69664 | tf_op jit(solution)/shard_map/ppermute | solution.py:365
  55.4 0.3 shard_map.83
  55.7 2.7 %collective-permute-start.12 = (bf16[144,256]{1,0:T(8,128)(2,1)S(1)}, bf16[144,256]{1,0:T(8,128)(2,1)S(1)}, u32[]{:S(2)}, u32[]{:S(2)}) collective-permute-start(bf16[144,256]{1,0:T(8,128)(2,1)S(1)} %get-tuple-element.30.mine), channel_id=1, source_target_pairs={{0,16},{4,20},{8,24},{12,28},{16,0},{20,4},{24,8},{28,12},{1,17},{... | collective-permute-start | bytes 221192 | tf_op jit(solution)/shard_map/ppermute | solution.py:371
  58.4 4.0 %collective-permute-done.12.other = bf16[144,256]{1,0:T(8,128)(2,1)S(1)} collective-permute-done((bf16[144,256]{1,0:T(8,128)(2,1)S(1)}, bf16[144,256]{1,0:T(8,128)(2,1)S(1)}, u32[]{:S(2)}, u32[]{:S(2)}) %collective-permute-start.12) | collective-permute-done | bytes 73760 | tf_op jit(solution)/shard_map/ppermute | solution.py:371
  62.3 1.0 %shard_map.84 = (bf16[4,8,128]{2,1,0:T(8,128)(2,1)}, bf16[4,128]{1,0:T(4,128)(2,1)}) custom-call(f32[8,256]{1,0:T(8,128)S(1)} %shard_map.77.asked, bf16[144,256]{1,0:T(8,128)(2,1)S(1)} %get-tuple-element.30.mine, bf16[144,256]{1,0:T(8,128)(2,1)S(1)} %collective-permute-done.12.other, f32[128,256]{1,0:T(8,128)S(1)} %get-tuple-element.31.exact), custom_call_target="tpu_custom_call" | custom-call | tf_op jit(solution)/shard_map/pallas_call | solution.py:372
  (18 shorter events, 0.0 us)
Async XLA Ops:
  0.6 32.8 %copy-start.6 = (f32[256]{0:T(256)S(1)}, f32[256]{0:T(256)}, u32[]{:S(2)}) copy-start(f32[256]{0:T(256)} %param.10) | copy-start | bytes 3076
  0.6 32.8 %copy-start.2 = (bf16[4096,256]{1,0:T(8,128)(2,1)S(1)}, bf16[4096,256]{1,0:T(8,128)(2,1)}, u32[]{:S(2)}) copy-start(bf16[4096,256]{1,0:T(8,128)(2,1)} %refs_4_.3) | copy-start | bytes 6291460
  0.6 32.8 %collective-permute-start.4 = (bf16[128,4096]{1,0:T(8,128)(2,1)}, bf16[128,4096]{1,0:T(8,128)(2,1)S(1)}, u32[]{:S(2)}, u32[]{:S(2)}) collective-permute-start(bf16[128,4096]{1,0:T(8,128)(2,1)} %tokens.3), channel_id=1, source_target_pairs={{0,1},{1,0},{2,3},{3,2},{4,5},{5,4},{6,7},{7,6},{8,9},{9,8},{10,11... | collective-permute-start | bytes 3145736 | tf_op jit(solution)/shard_map/ppermute | solution.py:314
  2.4 15.1 %collective-permute-start.7 = (bf16[64,4096]{1,0:T(8,128)(2,1)S(1)}, bf16[64,4096]{1,0:T(8,128)(2,1)S(1)}, u32[]{:S(2)}, u32[]{:S(2)}) collective-permute-start(bf16[64,4096]{1,0:T(8,128)(2,1)S(1)} %get-tuple-element.20), channel_id=1, source_target_pairs={{0,2},{1,3},{2,0},{3,1},{4,6},{5,7},{6,4},{7,5},{8,10},{9,11},{10,... | collective-permute-start | bytes 1572872 | tf_op jit(solution)/shard_map/ppermute | solution.py:313
  17.5 24.4 %collective-permute-start.8 = (bf16[64,4096]{1,0:T(8,128)(2,1)S(1)}, bf16[64,4096]{1,0:T(8,128)(2,1)S(1)}, u32[]{:S(2)}, u32[]{:S(2)}) collective-permute-start(bf16[64,4096]{1,0:T(8,128)(2,1)S(1)} %collective-permute-done.7.refs_2_), channel_id=1, source_target_pairs={{0,1},{1,0},{2,3},{3,2},{4,5},{5,4},{6,7},{7,6},{8,9},{9,8},{10,11... | collective-permute-start | bytes 1572872 | tf_op jit(solution)/shard_map/ppermute | solution.py:328
  18.5 14.4 %collective-permute-start.5 = (bf16[24,4096]{1,0:T(8,128)(2,1)S(1)}, bf16[24,4096]{1,0:T(8,128)(2,1)S(1)}, u32[]{:S(2)}, u32[]{:S(2)}) collective-permute-start(bf16[24,4096]{1,0:T(8,128)(2,1)S(1)} %shard_map.80), channel_id=1, source_target_pairs={{0,2},{1,3},{2,0},{3,1},{4,6},{5,7},{6,4},{7,5},{8,10},{9,11},{10,... | collective-permute-start | bytes 589832 | tf_op jit(solution)/shard_map/ppermute | solution.py:313
  20.3 13.1 %collective-permute-start = (bf16[24,4096]{1,0:T(8,128)(2,1)S(1)}, bf16[24,4096]{1,0:T(8,128)(2,1)S(1)}, u32[]{:S(2)}, u32[]{:S(2)}) collective-permute-start(bf16[24,4096]{1,0:T(8,128)(2,1)S(1)} %get-tuple-element.17), channel_id=1, source_target_pairs={{0,2},{1,3},{2,0},{3,1},{4,6},{5,7},{6,4},{7,5},{8,10},{9,11},{10,... | collective-permute-start | bytes 589832 | tf_op jit(solution)/shard_map/ppermute | solution.py:313
  20.6 12.3 %collective-permute-start.1 = (bf16[16,4096]{1,0:T(8,128)(2,1)S(1)}, bf16[16,4096]{1,0:T(8,128)(2,1)S(1)}, u32[]{:S(2)}, u32[]{:S(2)}) collective-permute-start(bf16[16,4096]{1,0:T(8,128)(2,1)S(1)} %get-tuple-element.18), channel_id=1, source_target_pairs={{0,2},{1,3},{2,0},{3,1},{4,6},{5,7},{6,4},{7,5},{8,10},{9,11},{10,... | collective-permute-start | bytes 393224 | tf_op jit(solution)/shard_map/ppermute | solution.py:313
  32.9 11.7 %collective-permute-start.3 = (bf16[16,4096]{1,0:T(8,128)(2,1)S(1)}, bf16[16,4096]{1,0:T(8,128)(2,1)S(1)}, u32[]{:S(2)}, u32[]{:S(2)}) collective-permute-start(bf16[16,4096]{1,0:T(8,128)(2,1)S(1)} %collective-permute-done.1.refs_1_), channel_id=1, source_target_pairs={{0,1},{1,0},{2,3},{3,2},{4,5},{5,4},{6,7},{7,6},{8,9},{9,8},{10,11... | collective-permute-start | bytes 393224 | tf_op jit(solution)/shard_map/ppermute | solution.py:328
  32.9 9.0 %collective-permute-start.6 = (bf16[24,4096]{1,0:T(8,128)(2,1)S(1)}, bf16[24,4096]{1,0:T(8,128)(2,1)S(1)}, u32[]{:S(2)}, u32[]{:S(2)}) collective-permute-start(bf16[24,4096]{1,0:T(8,128)(2,1)S(1)} %collective-permute-done.5.refs_0_), channel_id=1, source_target_pairs={{0,1},{1,0},{2,3},{3,2},{4,5},{5,4},{6,7},{7,6},{8,9},{9,8},{10,11... | collective-permute-start | bytes 589832 | tf_op jit(solution)/shard_map/ppermute | solution.py:328
  33.4 11.2 %collective-permute-start.2 = (bf16[24,4096]{1,0:T(8,128)(2,1)S(1)}, bf16[24,4096]{1,0:T(8,128)(2,1)S(1)}, u32[]{:S(2)}, u32[]{:S(2)}) collective-permute-start(bf16[24,4096]{1,0:T(8,128)(2,1)S(1)} %collective-permute-done.refs_0_), channel_id=1, source_target_pairs={{0,1},{1,0},{2,3},{3,2},{4,5},{5,4},{6,7},{7,6},{8,9},{9,8},{10,11... | collective-permute-start | bytes 589832 | tf_op jit(solution)/shard_map/ppermute | solution.py:328
  33.5 2.2 %copy-start = (bf16[4096,512]{1,0:T(8,128)(2,1)S(1)}, bf16[4096,512]{1,0:T(8,128)(2,1)}, u32[]{:S(2)}) copy-start(bf16[4096,512]{1,0:T(8,128)(2,1)} %refs_5_.3) | copy-start | bytes 12582916
  35.7 1.6 %copy-start.3 = (bf16[4096,256]{1,0:T(8,128)(2,1)S(1)}, bf16[4096,256]{1,0:T(8,128)(2,1)}, u32[]{:S(2)}) copy-start(bf16[4096,256]{1,0:T(8,128)(2,1)} %refs_6_.3) | copy-start | bytes 6291460
  37.3 1.2 %copy-start.5 = (bf16[128,4096]{1,0:T(8,128)(2,1)S(1)}, bf16[128,4096]{1,0:T(8,128)(2,1)}, u32[]{:S(2)}) copy-start(bf16[128,4096]{1,0:T(8,128)(2,1)} %tokens.3) | copy-start | bytes 3145732
  38.5 3.4 %copy-start.1 = (bf16[4096,512]{1,0:T(8,128)(2,1)S(1)}, bf16[4096,512]{1,0:T(8,128)(2,1)}, u32[]{:S(2)}) copy-start(bf16[4096,512]{1,0:T(8,128)(2,1)} %refs_5_.3) | copy-start | bytes 12582916
  38.5 3.4 %copy-start.4 = (bf16[4096,256]{1,0:T(8,128)(2,1)S(1)}, bf16[4096,256]{1,0:T(8,128)(2,1)}, u32[]{:S(2)}) copy-start(bf16[4096,256]{1,0:T(8,128)(2,1)} %refs_6_.3) | copy-start | bytes 6291460
  44.6 5.7 %copy-start.7 = (bf16[4,64]{1,0:T(4,128)(2,1)S(1)}, bf16[4,64]{1,0:T(4,128)(2,1)}, u32[]{:S(2)}) copy-start(bf16[4,64]{1,0:T(4,128)(2,1)} %question.1) | copy-start | bytes 1540
  46.8 4.6 %collective-permute-start.10 = (bf16[136,256]{1,0:T(8,128)(2,1)S(1)}, bf16[136,256]{1,0:T(8,128)(2,1)S(1)}, u32[]{:S(2)}, u32[]{:S(2)}) collective-permute-start(bf16[136,256]{1,0:T(8,128)(2,1)S(1)} %shard_map.82.refs_0_), channel_id=1, source_target_pairs={{0,8},{4,12},{8,0},{12,4},{16,24},{20,28},{24,16},{28,20},{1,9},{5... | collective-permute-start | bytes 208904 | tf_op jit(solution)/shard_map/ppermute | solution.py:365
  48.7 5.5 %collective-permute-start.11 = (bf16[136,256]{1,0:T(8,128)(2,1)S(1)}, bf16[136,256]{1,0:T(8,128)(2,1)S(1)}, u32[]{:S(2)}, u32[]{:S(2)}) collective-permute-start(bf16[136,256]{1,0:T(8,128)(2,1)S(1)} %shard_map.82.refs_0_), channel_id=1, source_target_pairs={{0,12},{4,8},{8,4},{12,0},{16,28},{20,24},{24,20},{28,16},{1,13},{... | collective-permute-start | bytes 208904 | tf_op jit(solution)/shard_map/ppermute | solution.py:365
  50.1 5.4 %collective-permute-start.9 = (bf16[136,256]{1,0:T(8,128)(2,1)S(1)}, bf16[136,256]{1,0:T(8,128)(2,1)S(1)}, u32[]{:S(2)}, u32[]{:S(2)}) collective-permute-start(bf16[136,256]{1,0:T(8,128)(2,1)S(1)} %shard_map.82.refs_0_), channel_id=1, source_target_pairs={{0,4},{4,0},{8,12},{12,8},{16,20},{20,16},{24,28},{28,24},{1,5},{5... | collective-permute-start | bytes 208904 | tf_op jit(solution)/shard_map/ppermute | solution.py:365
  55.7 6.6 %collective-permute-start.12 = (bf16[144,256]{1,0:T(8,128)(2,1)S(1)}, bf16[144,256]{1,0:T(8,128)(2,1)S(1)}, u32[]{:S(2)}, u32[]{:S(2)}) collective-permute-start(bf16[144,256]{1,0:T(8,128)(2,1)S(1)} %get-tuple-element.30.mine), channel_id=1, source_target_pairs={{0,16},{4,20},{8,24},{12,28},{16,0},{20,4},{24,8},{28,12},{1,17},{... | collective-permute-start | bytes 221192 | tf_op jit(solution)/shard_map/ppermute | solution.py:371
